TPU v7x, 32 devices: a whole 2x2x4 slice. The times are simulated.
32 devices in a mesh: sp: 8 (over z, y), tp: 4 (over x, core).
Axes of the slice: x: 2, y: 2, z: 4, core: 2. Of those that a mesh axis runs over, the one named last changes fastest.
Arguments:
- stream: bfloat16 [3072, 2048], P(('sp', 'tp')), may hold values from -6 to 6
- query_projected: bfloat16 [3072, 1024], P('sp', 'tp'), may hold values from -6 to 6
- key_projected: bfloat16 [3072, 1024], P('sp', 'tp'), may hold values from -6 to 6
- value_projected: bfloat16 [3072, 1024], P('sp', 'tp'), may hold values from -6 to 6
- gate_projected: bfloat16 [3072, 1024], P('sp', 'tp'), may hold values from -6 to 6
- strength_logits: bfloat16 [8, 3072], P('tp', 'sp'), may hold values from -7 to 4
- decay_preactivation: bfloat16 [8, 3072], P('tp', 'sp'), may hold values from -9 to 9
- extra_log_decay: float32 [8, 3072], P('tp', 'sp'), may hold values from -0.7 to 0
- head_decay_rate: float32 [8], P('tp'), may hold values from 0 to 0.1
- head_norm_gain: float32 [128], replicated, may hold values from 0.1 to 1.9
- head_output_matrix: bfloat16 [1024, 2048], P('tp'), may hold values from -0.1875 to 0.1875
- feed_norm_gain: float32 [2048], replicated, may hold values from 0.1 to 1.9
- gate_matrix: bfloat16 [2048, 5632], P('sp', 'tp'), may hold values from -0.125 to 0.125
- up_matrix: bfloat16 [2048, 5632], P('sp', 'tp'), may hold values from -0.125 to 0.125
- down_matrix: bfloat16 [5632, 2048], P('tp', 'sp'), may hold values from -0.078125 to 0.078125
Outputs:
- result: bfloat16 [3072, 2048], P(('sp', 'tp'))
All inputs are finite; a program needn't handle non-finite values.
Results may differ from a plain program's by a relative error of at most 0.015.
Values may be sent and summed in bfloat16 or wider, within the bound.
No kernel may reach another device: no remote copies, remote signals or barrier semaphores. Data moves between devices by JAX's collectives and lax.ppermute only.
A program may use at most 128 MiB of HBM per device.

v0:
```python
import jax
import jax.numpy as jnp
from jax import lax
from jax.sharding import PartitionSpec as P

HEAD = 128
BLOCK = 64


PRECISION_FULL = lax.Precision.HIGHEST
EPSILON = 1e-06


def from_behind(value, axis, by):
    size = lax.axis_size(axis)
    pairs = [(i, i + by) for i in range(size) if 0 <= i + by < size]
    return lax.ppermute(value, axis, pairs)


def unit_rows(tensor):
    return tensor * lax.rsqrt(jnp.sum(tensor * tensor, axis=-1, keepdims=True) + EPSILON)


def rms_scale(tensor):
    return tensor * lax.rsqrt(jnp.mean(tensor * tensor, axis=-1, keepdims=True) + EPSILON)


def block_correction(
    unit_queries,
    unit_keys,
    complete_values,
    strength_logits,
    decay_preactivation,
    extra_log_decay,
    head_decay_rate,
):
    head_count, length, head_width = unit_queries.shape
    block_count = length // BLOCK

    def to_blocks(tensor):
        return tensor.reshape((head_count, block_count, BLOCK) + tensor.shape[2:])

    beta_gate = jax.nn.sigmoid(strength_logits.astype(jnp.float32))
    decay_logarithm = (
        -head_decay_rate[:, None] * jax.nn.softplus(decay_preactivation.astype(jnp.float32))
        + extra_log_decay
    )
    query_block = to_blocks(unit_queries)
    key_block = to_blocks(unit_keys)
    value_block = to_blocks(complete_values)
    beta_block = to_blocks(beta_gate)
    cumulative = jnp.cumsum(to_blocks(decay_logarithm), axis=-1)
    causal = jnp.tril(jnp.ones((BLOCK, BLOCK), bool))
    strict = jnp.tril(jnp.ones((BLOCK, BLOCK), bool), -1)
    spread = cumulative[..., :, None] - cumulative[..., None, :]
    damping = jnp.where(causal, jnp.exp(jnp.where(causal, spread, 0.0)), 0.0)
    key_beta = key_block * beta_block[..., None]
    lower_part = jnp.einsum(
        "hnid,hnjd->hnij", key_beta, key_block, precision=PRECISION_FULL
    ) * jnp.where(strict, damping, 0.0)
    system = lower_part + jnp.eye(BLOCK, dtype=jnp.float32)
    right_side = jnp.concatenate(
        [value_block * beta_block[..., None], key_beta * jnp.exp(cumulative)[..., None]], axis=-1
    )
    solved = lax.linalg.triangular_solve(
        system, right_side, left_side=True, lower=True, unit_diagonal=True
    )
    target_values = solved[..., :head_width]
    householder_weights = solved[..., head_width:]
    inner_scores = (
        jnp.einsum("hnid,hnjd->hnij", query_block, key_block, precision=PRECISION_FULL) * damping
    )
    decayed_queries = query_block * jnp.exp(cumulative)[..., None]
    closing_log_decay = cumulative[..., -1:]
    decayed_keys = key_block * jnp.exp(closing_log_decay - cumulative)[..., None]
    return (
        decayed_queries,
        decayed_keys,
        target_values,
        householder_weights,
        inner_scores,
        closing_log_decay,
    )


def local_recurrence(
    query_projected,
    key_projected,
    value_projected,
    strength_logits,
    decay_preactivation,
    extra_log_decay,
    head_decay_rate,
):
    head_count = strength_logits.shape[0]
    tok_count = strength_logits.shape[1]

    def split_heads(tensor):
        return tensor.reshape(tok_count, head_count, HEAD).transpose(1, 0, 2).astype(jnp.float32)

    unit_queries = unit_rows(split_heads(query_projected)) * HEAD ** (-0.5)
    unit_keys = unit_rows(split_heads(key_projected))
    complete_values = split_heads(value_projected)
    score_terms = block_correction(
        unit_queries,
        unit_keys,
        complete_values,
        strength_logits,
        decay_preactivation,
        extra_log_decay,
        head_decay_rate,
    )
    identity = jnp.broadcast_to(jnp.eye(HEAD, dtype=jnp.float32), (head_count, HEAD, HEAD))

    def advance(carry, items):
        running_state, matrix_product = carry
        (
            decayed_queries,
            decayed_keys,
            target_values,
            householder_weights,
            inner_scores,
            closing_log_decay,
        ) = items
        new_state = target_values - jnp.einsum(
            "fdc,fcj->fdj", householder_weights, running_state, precision=PRECISION_FULL
        )
        layer_output = jnp.einsum(
            "fdc,fcj->fdj", decayed_queries, running_state, precision=PRECISION_FULL
        )
        layer_output = layer_output + jnp.einsum(
            "hij,hjv->hiv", inner_scores, new_state, precision=PRECISION_FULL
        )
        passed_state = decayed_queries - jnp.einsum(
            "hij,hjk->hik", inner_scores, householder_weights, precision=PRECISION_FULL
        )
        decay_span = jnp.einsum(
            "fdc,fcj->fdj", passed_state, matrix_product, precision=PRECISION_FULL
        )
        decay_factor = jnp.exp(closing_log_decay)[:, :, None]
        step_map = decay_factor * identity - jnp.einsum(
            "hik,hij->hkj", decayed_keys, householder_weights, precision=PRECISION_FULL
        )
        running_state = decay_factor * running_state + jnp.einsum(
            "xwp,xws->xps", decayed_keys, new_state, precision=PRECISION_FULL
        )
        matrix_product = jnp.einsum(
            "hij,hjk->hik", step_map, matrix_product, precision=PRECISION_FULL
        )
        return ((running_state, matrix_product), (layer_output, decay_span))

    moved = tuple((jnp.moveaxis(tensor, 1, 0) for tensor in score_terms))
    zeros_state = jnp.zeros((head_count, HEAD, HEAD), jnp.float32)
    (running_state, matrix_product), (block_outputs, decay_spans) = lax.scan(
        advance, (zeros_state, identity), moved
    )

    def merge_blocks(tensor):
        return jnp.moveaxis(tensor, 0, 1).reshape(head_count, tok_count, HEAD)

    return (
        merge_blocks(block_outputs),
        merge_blocks(decay_spans),
        matrix_product,
        running_state,
        identity,
    )


def feed_forward(whole_rows, gate_matrix, up_matrix, down_matrix):
    gate_whole, up_whole = (
        lax.all_gather(gate_matrix, "sp", axis=0, tiled=True),
        lax.all_gather(up_matrix, "sp", axis=0, tiled=True),
    )
    gate_total = jnp.dot(whole_rows, gate_whole, preferred_element_type=jnp.float32)
    up_total = jnp.dot(whole_rows, up_whole, preferred_element_type=jnp.float32)
    hidden = (jax.nn.silu(gate_total) * up_total).astype(jnp.bfloat16)
    down_whole = lax.all_gather(down_matrix, "sp", axis=1, tiled=True)
    return jnp.dot(hidden, down_whole, preferred_element_type=jnp.float32)


def body(
    stream,
    query_projected,
    key_projected,
    value_projected,
    gate_projected,
    strength_logits,
    decay_preactivation,
    extra_log_decay,
    head_decay_rate,
    head_norm_gain,
    head_output_matrix,
    feed_norm_gain,
    gate_matrix,
    up_matrix,
    down_matrix,
):
    block_outputs, decay_spans, matrix_product, running_state, identity = local_recurrence(
        query_projected,
        key_projected,
        value_projected,
        strength_logits,
        decay_preactivation,
        extra_log_decay,
        head_decay_rate,
    )
    zeros_state = jnp.zeros_like(running_state)

    def pass_state(turn, state_inflow):
        leaving = (
            jnp.einsum("hij,hjk->hik", matrix_product, state_inflow, precision=PRECISION_FULL)
            + running_state
        )
        return from_behind(leaving.astype(jnp.bfloat16), "sp", 1).astype(leaving.dtype)

    state_inflow = lax.fori_loop(0, lax.axis_size("sp") - 1, pass_state, zeros_state)
    attention_output = block_outputs + jnp.einsum(
        "qwc,qcn->qwn", decay_spans, state_inflow, precision=PRECISION_FULL
    )
    head_count = attention_output.shape[0]
    tok_count = attention_output.shape[1]
    normed_heads = rms_scale(attention_output) * head_norm_gain
    gated = normed_heads.transpose(1, 0, 2).reshape(tok_count, head_count * HEAD)
    mixed = (gated * jax.nn.silu(gate_projected.astype(jnp.float32))).astype(jnp.bfloat16)
    branch = lax.psum_scatter(
        jnp.dot(mixed, head_output_matrix, preferred_element_type=jnp.float32).astype(jnp.bfloat16),
        "tp",
        scatter_dimension=0,
        tiled=True,
    ).astype(jnp.float32)
    residual_own = stream.astype(jnp.float32) + branch
    normed_own = (rms_scale(residual_own) * feed_norm_gain).astype(jnp.bfloat16)
    whole_rows = lax.all_gather(normed_own, "tp", axis=0, tiled=True)
    ffn_term = feed_forward(whole_rows, gate_matrix, up_matrix, down_matrix)
    ffn_own = lax.psum_scatter(
        ffn_term.astype(jnp.bfloat16), "tp", scatter_dimension=0, tiled=True
    ).astype(jnp.float32)
    return (residual_own + ffn_own).astype(jnp.bfloat16)


def solution(mesh):
    placed = (
        P(("sp", "tp"), None),
        P("sp", "tp"),
        P("sp", "tp"),
        P("sp", "tp"),
        P("sp", "tp"),
        P("tp", "sp"),
        P("tp", "sp"),
        P("tp", "sp"),
        P("tp"),
        P(),
        P("tp", None),
        P(),
        P("sp", "tp"),
        P("sp", "tp"),
        P("tp", "sp"),
    )
    return jax.shard_map(
        body, mesh=mesh, in_specs=placed, out_specs=P(("sp", "tp"), None), check_vma=False
    )
```

profile of v0, /device:TPU:0, one launch (start us, length us, event | category | flops | bytes accessed | tf_op | source)
XLA Modules:
  0.0 551.2 jit_solution(7347479485389619198)
XLA Ops:
  8.9 1.1 fusion.64
  10.0 1.1 fusion.62
  11.1 1.1 fusion.60
  12.2 1.1 fusion.61
  16.0 59.6 %custom-call.3 = f32[2,6,1,64,64]{3,4,2,1,0:T(8,128)} custom-call(f32[2,6,1,64,64]{4,3,2,1,0:T(8,128)S(1)} %fusion.48), custom_call_target="InvertDiagBlocksLowerTriangular" | custom-call | tf_op jit(solution)/shard_map/triangular_solve | solution.py:65
  75.6 1.1 multiply_multiply_fusion
  79.3 36.4 %while.28 = (s32[]{:T(128)}, f32[2,128,128]{2,1,0:T(8,128)S(1)}, f32[2,128,128]{2,1,0:T(8,128)S(1)}, f32[6,2,64,128]{3,2,0,1:T(8,128)}, f32[6,2,64,128]{3,2,0,1:...) while((s32[]{:T(128)}, f32[2,128,128]{2,1,0:T(8,128)S(1)}, ...), condition=%wide.region_4.5_spmd.clone, body=%wide.region_3.4_spmd.clone.sunk | while | flops 201605120 | bytes 2759337 | solution.py:154
  79.4 1.1 convolution_subtract_fusion.6
  80.5 1.1 fusion.145
  85.4 1.1 convolution_subtract_fusion.6
  86.5 1.1 fusion.145
  91.5 1.1 convolution_subtract_fusion.6
  92.6 1.1 fusion.145
  97.5 1.1 convolution_subtract_fusion.6
  98.6 1.1 fusion.145
  103.6 1.1 convolution_subtract_fusion.6
  104.7 1.1 fusion.145
  109.7 1.1 convolution_subtract_fusion.6
  110.7 1.1 fusion.145
  113.1 1.0 convolution_subtract_fusion.8
  115.7 1.2 copy.42
  116.9 49.8 %while.29 = (s32[]{:T(128)}, f32[2,128,128]{2,1,0:T(8,128)S(1)}, f32[2,128,128]{2,1,0:T(8,128)S(1)}, f32[2,128,128]{2,1,0:T(8,128)S(1)}, s32[]{:T(128)}, /*index=5*/s32[]{:T(128)}) while((s32[]{:T(128)}, f32[2,128,128]{2,1,0:T(8,128)S(1)}, f32[2,128,128]{2,1,0:T(8,128)S(1)}, f32[2,128,128]{2,1,0:T(8,128)S(1)}, s32[]{:T(128)}, ...), condition=%wide.region_6.7_spmd.clone, body=%wide.region_5.6_spmd.clone.sunk | while | flops 50462720 | bytes 917623 | solution.py:217
  117.2 4.9 collective-permute-start
  122.1 1.9 collective-permute-done
  124.3 4.3 collective-permute-start
  128.6 1.9 collective-permute-done
  130.8 4.3 collective-permute-start
  135.1 1.9 collective-permute-done
  137.3 5.2 collective-permute-start
  142.5 1.9 collective-permute-done
  144.7 5.2 collective-permute-start
  149.9 1.9 collective-permute-done
  152.1 5.3 collective-permute-start
  157.3 2.1 collective-permute-done
  159.7 5.1 collective-permute-start
  164.8 1.9 collective-permute-done
  167.8 1.8 convolution_convert_fusion.1
  169.6 31.9 %reduce-scatter.3.cloned.1.call-done = bf16[96,2048]{1,0:T(8,128)(2,1)} async-done(((bf16[384,2048]{1,0:T(8,128)(2,1)}), bf16[96,2048]{1,0:T(8,128)(2,1)}) %reduce-scatter.3.cloned.1.call-update) | async-done | bytes 393232 | tf_op jit(solution)/shard_map/reduce_scatter | solution.py:226
  201.5 1.2 multiply_reduce_fusion
  202.8 1.9 multiply_convert_fusion
  206.8 17.7 %all-gather.5.cloned.1.call-done = bf16[384,2048]{1,0:T(8,128)(2,1)} async-done(((bf16[96,2048]{1,0:T(8,128)(2,1)}), bf16[384,2048]{1,0:T(8,128)(2,1)}) %all-gather.5.cloned.1.call-update) | async-done | bytes 1572880 | tf_op jit(solution)/shard_map/all_gather | solution.py:234
  224.5 94.5 %all-gather.7.cloned.1.call-done = bf16[2048,1408]{1,0:T(8,128)(2,1)} async-done(((bf16[256,1408]{1,0:T(8,128)(2,1)}), bf16[2048,1408]{1,0:T(8,128)(2,1)}) %all-gather.7.cloned.1.call-update) | async-done | bytes 5767184 | tf_op jit(solution)/shard_map/all_gather | solution.py:172
  319.0 7.1 %fusion.84 = f32[384,1408]{1,0:T(8,128)} fusion(bf16[384,2048]{1,0:T(8,128)(2,1)} %all-gather.5.cloned.1.call-done, bf16[2048,1408]{1,0:T(8,128)(2,1)} %all-gather.7.cloned.1.call-done), kind=kOutput, calls=%fused_computation.133 | convolution fusion | flops 2214592512 | bytes 9502720 | tf_op jit(solution)/shard_map/dot_general | solution.py:175
  326.1 86.2 %all-gather.11.cloned.1.call-done = bf16[1408,2048]{1,0:T(8,128)(2,1)} async-done(((bf16[1408,256]{1,0:T(8,128)(2,1)}), bf16[1408,2048]{1,0:T(8,128)(2,1)}) %all-gather.11.cloned.1.call-update) | async-done | bytes 5767184 | tf_op jit(solution)/shard_map/all_gather | solution.py:178
  412.3 92.6 %all-gather.9.cloned.1.call-done = bf16[2048,1408]{1,0:T(8,128)(2,1)} async-done(((bf16[256,1408]{1,0:T(8,128)(2,1)}), bf16[2048,1408]{1,0:T(8,128)(2,1)}) %all-gather.9.cloned.1.call-update) | async-done | bytes 5767184 | tf_op jit(solution)/shard_map/all_gather | solution.py:173
  504.8 11.3 %convolution_convert_fusion = bf16[384,2048]{1,0:T(8,128)(2,1)} fusion(bf16[1408,2048]{1,0:T(8,128)(2,1)} %all-gather.11.cloned.1.call-done, bf16[384,2048]{1,0:T(8,128)(2,1)S(1)} %copy-done.7, bf16[2048,1408]{1,0:T(8,128)(2,1)} %all-gather.9.cloned.1.call-done, f32[384,1408]{1,0:T(8,128)} %fusion.84), kind=kOutput, calls=%fused_computation.52 | convolution fusion | flops 4433215488 | bytes 16842752 | tf_op jit(solution)/shard_map/dot_general | solution.py:179
  516.1 26.4 %reduce-scatter.5.cloned.1.call-done = bf16[96,2048]{1,0:T(8,128)(2,1)} async-done(((bf16[384,2048]{1,0:T(8,128)(2,1)}), bf16[96,2048]{1,0:T(8,128)(2,1)}) %reduce-scatter.5.cloned.1.call-update) | async-done | bytes 393232 | tf_op jit(solution)/shard_map/reduce_scatter | solution.py:236
  542.5 1.9 add_convert_fusion
  (121 shorter events, 34.4 us)
Async XLA Ops:
  6.5 161.2 %copy-start = (bf16[256,2048]{1,0:T(8,128)(2,1)S(1)}, bf16[256,2048]{1,0:T(8,128)(2,1)}, u32[]{:S(2)}) copy-start(bf16[256,2048]{1,0:T(8,128)(2,1)} %param.29) | copy-start | bytes 3145732
  6.5 195.0 %reduce-scatter.3.cloned.1.call-start = ((), (), s32[]{:S(2)}) async-start(), calls=%async_computation.2 | async-start | bytes 1966080 | tf_op jit(solution)/shard_map/reduce_scatter | solution.py:226
  75.6 1.1 copy-start.4
  115.7 51.0 %copy-start.3 = (f32[6,2,64,128]{3,2,0,1:T(8,128)S(1)}, f32[6,2,64,128]{3,2,0,1:T(8,128)}, u32[]{:S(2)}) copy-start(f32[6,2,64,128]{3,2,0,1:T(8,128)} %get-tuple-element.93) | copy-start | bytes 1179652
  116.9 50.5 %copy-start.6 = (f32[128]{0:T(128)S(1)}, f32[128]{0:T(128)}, u32[]{:S(2)}) copy-start(f32[128]{0:T(128)} %param.28) | copy-start | bytes 1540
  117.2 6.8 %collective-permute-start = (bf16[2,128,128]{2,1,0:T(8,128)(2,1)S(1)}, bf16[2,128,128]{2,1,0:T(8,128)(2,1)S(1)}, u32[]{:S(2)}, u32[]{:S(2)}) collective-permute-start(bf16[2,128,128]{2,1,0:T(8,128)(2,1)S(1)} %fusion.150), channel_id=1, source_target_pairs={{0,4},{4,8},{8,12},{12,16},{16,20},{20,24},{24,28},{1,5},{5,9},{9,... | collective-permute-start | bytes 196616 | tf_op jit(solution)/shard_map/while/body/eval_jaxpr/ppermute | solution.py:17
  124.3 6.2 %collective-permute-start = (bf16[2,128,128]{2,1,0:T(8,128)(2,1)S(1)}, bf16[2,128,128]{2,1,0:T(8,128)(2,1)S(1)}, u32[]{:S(2)}, u32[]{:S(2)}) collective-permute-start(bf16[2,128,128]{2,1,0:T(8,128)(2,1)S(1)} %fusion.150), channel_id=1, source_target_pairs={{0,4},{4,8},{8,12},{12,16},{16,20},{20,24},{24,28},{1,5},{5,9},{9,... | collective-permute-start | bytes 196616 | tf_op jit(solution)/shard_map/while/body/eval_jaxpr/ppermute | solution.py:17
  130.8 6.2 %collective-permute-start = (bf16[2,128,128]{2,1,0:T(8,128)(2,1)S(1)}, bf16[2,128,128]{2,1,0:T(8,128)(2,1)S(1)}, u32[]{:S(2)}, u32[]{:S(2)}) collective-permute-start(bf16[2,128,128]{2,1,0:T(8,128)(2,1)S(1)} %fusion.150), channel_id=1, source_target_pairs={{0,4},{4,8},{8,12},{12,16},{16,20},{20,24},{24,28},{1,5},{5,9},{9,... | collective-permute-start | bytes 196616 | tf_op jit(solution)/shard_map/while/body/eval_jaxpr/ppermute | solution.py:17
  137.3 7.1 %collective-permute-start = (bf16[2,128,128]{2,1,0:T(8,128)(2,1)S(1)}, bf16[2,128,128]{2,1,0:T(8,128)(2,1)S(1)}, u32[]{:S(2)}, u32[]{:S(2)}) collective-permute-start(bf16[2,128,128]{2,1,0:T(8,128)(2,1)S(1)} %fusion.150), channel_id=1, source_target_pairs={{0,4},{4,8},{8,12},{12,16},{16,20},{20,24},{24,28},{1,5},{5,9},{9,... | collective-permute-start | bytes 196616 | tf_op jit(solution)/shard_map/while/body/eval_jaxpr/ppermute | solution.py:17
  144.7 7.1 %collective-permute-start = (bf16[2,128,128]{2,1,0:T(8,128)(2,1)S(1)}, bf16[2,128,128]{2,1,0:T(8,128)(2,1)S(1)}, u32[]{:S(2)}, u32[]{:S(2)}) collective-permute-start(bf16[2,128,128]{2,1,0:T(8,128)(2,1)S(1)} %fusion.150), channel_id=1, source_target_pairs={{0,4},{4,8},{8,12},{12,16},{16,20},{20,24},{24,28},{1,5},{5,9},{9,... | collective-permute-start | bytes 196616 | tf_op jit(solution)/shard_map/while/body/eval_jaxpr/ppermute | solution.py:17
  152.1 7.4 %collective-permute-start = (bf16[2,128,128]{2,1,0:T(8,128)(2,1)S(1)}, bf16[2,128,128]{2,1,0:T(8,128)(2,1)S(1)}, u32[]{:S(2)}, u32[]{:S(2)}) collective-permute-start(bf16[2,128,128]{2,1,0:T(8,128)(2,1)S(1)} %fusion.150), channel_id=1, source_target_pairs={{0,4},{4,8},{8,12},{12,16},{16,20},{20,24},{24,28},{1,5},{5,9},{9,... | collective-permute-start | bytes 196616 | tf_op jit(solution)/shard_map/while/body/eval_jaxpr/ppermute | solution.py:17
  159.7 7.0 %collective-permute-start = (bf16[2,128,128]{2,1,0:T(8,128)(2,1)S(1)}, bf16[2,128,128]{2,1,0:T(8,128)(2,1)S(1)}, u32[]{:S(2)}, u32[]{:S(2)}) collective-permute-start(bf16[2,128,128]{2,1,0:T(8,128)(2,1)S(1)} %fusion.150), channel_id=1, source_target_pairs={{0,4},{4,8},{8,12},{12,16},{16,20},{20,24},{24,28},{1,5},{5,9},{9,... | collective-permute-start | bytes 196616 | tf_op jit(solution)/shard_map/while/body/eval_jaxpr/ppermute | solution.py:17
  166.7 1.0 copy-start.8
  167.7 33.8 %copy-start.1 = (bf16[96,2048]{1,0:T(8,128)(2,1)S(1)}, bf16[96,2048]{1,0:T(8,128)(2,1)}, u32[]{:S(2)}) copy-start(bf16[96,2048]{1,0:T(8,128)(2,1)} %param.19) | copy-start | bytes 1179652
  167.7 35.0 %copy-start.5 = (f32[2048]{0:T(1024)S(1)}, f32[2048]{0:T(1024)}, u32[]{:S(2)}) copy-start(f32[2048]{0:T(1024)} %param.30) | copy-start | bytes 24580
  169.6 54.9 %all-gather.5.cloned.1.call-start = ((), (), s32[]{:S(2)}) async-start(), calls=%async_computation.3 | async-start | bytes 1966080 | tf_op jit(solution)/shard_map/all_gather | solution.py:234
  204.7 114.3 %all-gather.7.cloned.1.call-start = ((), (), s32[]{:S(2)}) async-start(), calls=%async_computation.4 | async-start | bytes 6488064 | tf_op jit(solution)/shard_map/all_gather | solution.py:172
  205.4 206.8 %all-gather.11.cloned.1.call-start = ((), (), s32[]{:S(2)}) async-start(), calls=%async_computation.6 | async-start | bytes 6488064 | tf_op jit(solution)/shard_map/all_gather | solution.py:178
  206.0 298.8 %all-gather.9.cloned.1.call-start = ((), (), s32[]{:S(2)}) async-start(), calls=%async_computation.5 | async-start | bytes 6488064 | tf_op jit(solution)/shard_map/all_gather | solution.py:173
  206.6 335.9 %reduce-scatter.5.cloned.1.call-start = ((), (), s32[]{:S(2)}) async-start(), calls=%async_computation.7 | async-start | bytes 1966080 | tf_op jit(solution)/shard_map/reduce_scatter | solution.py:236
  224.5 280.3 %copy-start.7 = (bf16[384,2048]{1,0:T(8,128)(2,1)S(1)}, bf16[384,2048]{1,0:T(8,128)(2,1)}, u32[]{:S(2)}) copy-start(bf16[384,2048]{1,0:T(8,128)(2,1)} %all-gather.5.cloned.1.call-done) | copy-start | bytes 4718596
  326.1 216.4 %copy-start.2 = (bf16[96,2048]{1,0:T(8,128)(2,1)S(1)}, bf16[96,2048]{1,0:T(8,128)(2,1)}, u32[]{:S(2)}) copy-start(bf16[96,2048]{1,0:T(8,128)(2,1)} %reduce-scatter.3.cloned.1.call-done) | copy-start | bytes 1179652
Sparse Core Ops, SparseCore 0:
  169.7 31.7 reduce-scatter.2
  204.8 19.6 all-gather.4
  226.7 92.3 all-gather.6
  320.9 91.2 all-gather.10
  414.3 90.4 all-gather.8
  516.2 26.1 reduce-scatter.4
where the time goes:
time: 553 us; the launch traced here: 551 us
  waiting for transfers between devices  364 us (66%)
  other arithmetic  74.1 us (13%)
  matrix products  60.9 us (11%)
  starting transfers between devices  34.5 us (6%)
  between operations  13.7 us (2%)
    all_gather x1, waiting for transfers between devices, feed_forward(): lax.all_gather(gate_matrix, 'sp', axis=0, tiled=True)  94.5 us
    all_gather x1, waiting for transfers between devices, feed_forward(): lax.all_gather(up_matrix, 'sp', axis=0, tiled=True)  92.6 us
    all_gather x1, waiting for transfers between devices, feed_forward(): down_whole = lax.all_gather(down_matrix, 'sp', axis=1, tiled=True)  86.2 us
    another operation x2, other arithmetic, block_correction(): lax.linalg.triangular_solve(system, right_side, left_side=True, lower=Tru...  59.6 us
    ppermute x7, starting transfers between devices, from_behind(): return lax.ppermute(value, axis, pairs)  34.2 us
    reduce_scatter x1, waiting for transfers between devices, body(): lax.psum_scatter(jnp.dot(mixed, head_output_matrix, preferred_element_typ...  31.9 us
    reduce_scatter x1, waiting for transfers between devices, body(): lax.psum_scatter(ffn_term.astype(jnp.bfloat16), 'tp', scatter_dimension=0...  26.4 us
    all_gather x1, waiting for transfers between devices, body(): whole_rows = lax.all_gather(normed_own, 'tp', axis=0, tiled=True)  17.7 us
  transfers between devices with their start and end apart: 13, of which 13 were waited for; matrix products, arithmetic and copies ran while one was open for 1% of the time, Pallas kernels for 0%

commit v1 on v0

--- a/solution.py
+++ b/solution.py
@@ -23,6 +23,86 @@
 
 def rms_scale(tensor):
     return tensor * lax.rsqrt(jnp.mean(tensor * tensor, axis=-1, keepdims=True) + EPSILON)
+
+
+def unit_lower_inverse(strict_lower):
+    size = strict_lower.shape[-1]
+    row = jnp.arange(size)[:, None]
+    column = jnp.arange(size)[None, :]
+
+    def corner(half):
+        same_pair = row // (2 * half) == column // (2 * half)
+        return jnp.where(same_pair & (row // half != column // half), strict_lower, 0.0)
+
+    inverse = jnp.eye(size, dtype=jnp.float32) - corner(1)
+    half = 2
+    while half < size:
+        left = jnp.einsum("hnij,hnjk->hnik", inverse, corner(half), precision=PRECISION_FULL)
+        inverse = inverse - jnp.einsum(
+            "hnij,hnjk->hnik", left, inverse, precision=PRECISION_FULL
+        )
+        half *= 2
+    return inverse
+
+
+def swap(value, axis, bit):
+    size = lax.axis_size(axis)
+    return lax.ppermute(value, axis, [(i, i ^ bit) for i in range(size)])
+
+
+def relative_order(count):
+    order = [0]
+    bit = count // 2
+    while bit:
+        order = order + [place ^ bit for place in order]
+        bit //= 2
+    return order
+
+
+def gather_relative(own):
+    bit = lax.axis_size("tp") // 2
+    while bit:
+        own = jnp.concatenate([own, swap(own, "tp", bit)], axis=0)
+        bit //= 2
+    return own
+
+
+def scatter_relative(left_rows, matrix):
+    size = lax.axis_size("tp")
+    if size == 1:
+        return jnp.dot(left_rows, matrix, preferred_element_type=jnp.float32)
+    half = left_rows.shape[0] // 2
+    leaving = jnp.dot(left_rows[half:], matrix, preferred_element_type=jnp.float32)
+    arrived = swap(leaving.astype(jnp.bfloat16), "tp", 1)
+    total = jnp.dot(left_rows[:half], matrix, preferred_element_type=jnp.float32)
+    total = total + arrived.astype(jnp.float32)
+    bit = 2
+    while bit < size:
+        half = total.shape[0] // 2
+        arrived = swap(total[half:].astype(jnp.bfloat16), "tp", bit)
+        total = total[:half] + arrived.astype(jnp.float32)
+        bit *= 2
+    return total
+
+
+def inflow_of_earlier(matrix_product, running_state):
+    size = lax.axis_size("sp")
+    width = running_state.shape[-1]
+    pair = jnp.concatenate([matrix_product, running_state], axis=-1)
+    pair = from_behind(pair.astype(jnp.bfloat16), "sp", 1).astype(jnp.float32)
+    by = 1
+    while by < size - 1:
+        matrix, state = pair[..., :width], pair[..., width:]
+        last = 2 * by >= size - 1
+        sent = (state if last else pair).astype(jnp.bfloat16)
+        earlier = from_behind(sent, "sp", by).astype(jnp.float32)
+        moved = jnp.einsum("hij,hjk->hik", matrix, earlier, precision=PRECISION_FULL)
+        if last:
+            pair = jnp.concatenate([matrix, state + moved], axis=-1)
+        else:
+            pair = jnp.concatenate([moved[..., :width], state + moved[..., width:]], axis=-1)
+        by *= 2
+    return pair[..., width:]
 
 
 def block_correction(
@@ -58,12 +138,11 @@
     lower_part = jnp.einsum(
         "hnid,hnjd->hnij", key_beta, key_block, precision=PRECISION_FULL
     ) * jnp.where(strict, damping, 0.0)
-    system = lower_part + jnp.eye(BLOCK, dtype=jnp.float32)
     right_side = jnp.concatenate(
         [value_block * beta_block[..., None], key_beta * jnp.exp(cumulative)[..., None]], axis=-1
     )
-    solved = lax.linalg.triangular_solve(
-        system, right_side, left_side=True, lower=True, unit_diagonal=True
+    solved = jnp.einsum(
+        "hnij,hnjd->hnid", unit_lower_inverse(lower_part), right_side, precision=PRECISION_FULL
     )
     target_values = solved[..., :head_width]
     householder_weights = solved[..., head_width:]
@@ -165,18 +244,6 @@
         running_state,
         identity,
     )
-
-
-def feed_forward(whole_rows, gate_matrix, up_matrix, down_matrix):
-    gate_whole, up_whole = (
-        lax.all_gather(gate_matrix, "sp", axis=0, tiled=True),
-        lax.all_gather(up_matrix, "sp", axis=0, tiled=True),
-    )
-    gate_total = jnp.dot(whole_rows, gate_whole, preferred_element_type=jnp.float32)
-    up_total = jnp.dot(whole_rows, up_whole, preferred_element_type=jnp.float32)
-    hidden = (jax.nn.silu(gate_total) * up_total).astype(jnp.bfloat16)
-    down_whole = lax.all_gather(down_matrix, "sp", axis=1, tiled=True)
-    return jnp.dot(hidden, down_whole, preferred_element_type=jnp.float32)
 
 
 def body(
@@ -196,7 +263,10 @@
     up_matrix,
     down_matrix,
 ):
-    block_outputs, decay_spans, matrix_product, running_state, identity = local_recurrence(
+    gate_whole = lax.all_gather(gate_matrix, "sp", axis=0, tiled=True)
+    up_whole = lax.all_gather(up_matrix, "sp", axis=0, tiled=True)
+    down_whole = lax.all_gather(down_matrix, "sp", axis=1, tiled=True)
+    block_outputs, decay_spans, matrix_product, running_state, _ = local_recurrence(
         query_projected,
         key_projected,
         value_projected,
@@ -205,16 +275,7 @@
         extra_log_decay,
         head_decay_rate,
     )
-    zeros_state = jnp.zeros_like(running_state)
-
-    def pass_state(turn, state_inflow):
-        leaving = (
-            jnp.einsum("hij,hjk->hik", matrix_product, state_inflow, precision=PRECISION_FULL)
-            + running_state
-        )
-        return from_behind(leaving.astype(jnp.bfloat16), "sp", 1).astype(leaving.dtype)
-
-    state_inflow = lax.fori_loop(0, lax.axis_size("sp") - 1, pass_state, zeros_state)
+    state_inflow = inflow_of_earlier(matrix_product, running_state)
     attention_output = block_outputs + jnp.einsum(
         "qwc,qcn->qwn", decay_spans, state_inflow, precision=PRECISION_FULL
     )
@@ -223,19 +284,24 @@
     normed_heads = rms_scale(attention_output) * head_norm_gain
     gated = normed_heads.transpose(1, 0, 2).reshape(tok_count, head_count * HEAD)
     mixed = (gated * jax.nn.silu(gate_projected.astype(jnp.float32))).astype(jnp.bfloat16)
-    branch = lax.psum_scatter(
-        jnp.dot(mixed, head_output_matrix, preferred_element_type=jnp.float32).astype(jnp.bfloat16),
-        "tp",
-        scatter_dimension=0,
-        tiled=True,
-    ).astype(jnp.float32)
+    tp_size = lax.axis_size("tp")
+    tp_index = lax.axis_index("tp")
+    chunks = mixed.reshape(tp_size, tok_count // tp_size, head_count * HEAD)
+    ordered = jnp.concatenate(
+        [
+            lax.dynamic_index_in_dim(chunks, tp_index ^ place, 0, keepdims=False)
+            for place in relative_order(tp_size)
+        ],
+        axis=0,
+    )
+    branch = scatter_relative(ordered, head_output_matrix)
     residual_own = stream.astype(jnp.float32) + branch
     normed_own = (rms_scale(residual_own) * feed_norm_gain).astype(jnp.bfloat16)
-    whole_rows = lax.all_gather(normed_own, "tp", axis=0, tiled=True)
-    ffn_term = feed_forward(whole_rows, gate_matrix, up_matrix, down_matrix)
-    ffn_own = lax.psum_scatter(
-        ffn_term.astype(jnp.bfloat16), "tp", scatter_dimension=0, tiled=True
-    ).astype(jnp.float32)
+    whole_rows = gather_relative(normed_own)
+    gate_total = jnp.dot(whole_rows, gate_whole, preferred_element_type=jnp.float32)
+    up_total = jnp.dot(whole_rows, up_whole, preferred_element_type=jnp.float32)
+    hidden = (jax.nn.silu(gate_total) * up_total).astype(jnp.bfloat16)
+    ffn_own = scatter_relative(hidden, down_whole)
     return (residual_own + ffn_own).astype(jnp.bfloat16)
 
 

time: 553 us -> 327 us (0.59)
  waiting for transfers between devices: 364 us -> 212 us
  other arithmetic: 74.1 us -> 3.82 us
    all_gather x4 -> x3, waiting for transfers between devices: 291 us -> 153 us  [the longest x1 86 us: body(): down_whole = lax.all_gather(down_matrix, 'sp', axis=1, tiled=True)]
    another operation x4 -> x5, other arithmetic: 59.7 us -> 0.04 us  [the longest x2 59.6 us: block_correction(): lax.linalg.triangular_solve(system, right_side, left_side=True, lower=Tru...]
    reduce_scatter x2 -> x0, waiting for transfers between devices: 58.3 us -> none  [the longest x1 31.9 us: body(): lax.psum_scatter(jnp.dot(mixed, head_output_matrix, preferred_element_typ...]
    ppermute x0 -> x6, waiting for transfers between devices: none -> 37.2 us  [swap(): return lax.ppermute(value, axis, [(i, i ^ bit) for i in range(size)])]
    ppermute x7 -> x4, waiting for transfers between devices: 13.4 us -> 19.2 us  [from_behind(): return lax.ppermute(value, axis, pairs)]
    dot_general x10 -> x20, matrix products: 22 us -> 27.7 us  [the longest x1 7.38 us: body(): up_total = jnp.dot(whole_rows, up_whole, preferred_element_type=jnp.float32)]
    ppermute x7 -> x4, starting transfers between devices: 34.2 us -> 35.9 us  [from_behind(): return lax.ppermute(value, axis, pairs)]
  transfers between devices with their start and end apart: 13 -> 13, of which waited for: 13 -> 12; matrix products, arithmetic and copies ran while one was open for 1% -> 17% of each run, Pallas kernels for 0% -> 0%
where the time goes in v1:
time: 327 us; the launch traced here: 326 us
  waiting for transfers between devices  212 us (65%)
  matrix products  55.6 us (17%)
  starting transfers between devices  38.3 us (12%)
  between operations  13.8 us (4%)
  other arithmetic  3.82 us (1%)
    all_gather x1, waiting for transfers between devices, body(): down_whole = lax.all_gather(down_matrix, 'sp', axis=1, tiled=True)  86 us
    all_gather x1, waiting for transfers between devices, body(): up_whole = lax.all_gather(up_matrix, 'sp', axis=0, tiled=True)  67.4 us
    ppermute x6, waiting for transfers between devices, swap(): return lax.ppermute(value, axis, [(i, i ^ bit) for i in range(size)])  37.2 us
    ppermute x4, starting transfers between devices, from_behind(): return lax.ppermute(value, axis, pairs)  35.9 us
    ppermute x4, waiting for transfers between devices, from_behind(): return lax.ppermute(value, axis, pairs)  19.2 us
    dot_general x1, matrix products, body(): up_total = jnp.dot(whole_rows, up_whole, preferred_element_type=jnp.float32)  7.38 us
    dot_general x1, matrix products, body(): jnp.dot(whole_rows, gate_whole, preferred_element_type=jnp.float32)  7.12 us
  transfers between devices with their start and end apart: 13, of which 12 were waited for; matrix products, arithmetic and copies ran while one was open for 17% of the time, Pallas kernels for 0%

profile of v1, /device:TPU:0, one launch (start us, length us, event | category | flops | bytes accessed | tf_op | source)
XLA Modules:
  0.0 326.3 jit_solution(2462705551969413879)
XLA Ops:
  6.6 0.7 all-gather.4.cloned.1.call-update
  7.3 0.7 all-gather.6.cloned.1.call-update
  8.1 0.7 all-gather.8.cloned.1.call-update
  10.2 0.8 convolution_multiply_fusion
  17.4 0.8 fusion.42
  18.3 0.8 slice_bitcast_fusion
  19.1 0.8 fusion.38
  20.0 26.2 %while.17 = (s32[]{:T(128)}, f32[2,128,128]{2,1,0:T(8,128)S(1)}, f32[2,128,128]{2,1,0:T(8,128)S(1)}, f32[6,2,64,128]{3,2,0,1:T(8,128)}, f32[6,2,64,128]{3,2,0,1:...) while((s32[]{:T(128)}, f32[2,128,128]{2,1,0:T(8,128)S(1)}, ...), condition=%wide.region_4.5_spmd.clone, body=%wide.region_3.4_spmd.clone.sunk | while | flops 201605120 | bytes 2758829 | solution.py:233
  20.0 1.1 convolution_subtract_fusion.11
  21.4 0.8 fusion.205
  22.8 0.9 fusion.206
  24.4 1.1 convolution_subtract_fusion.11
  25.7 0.8 fusion.205
  27.2 0.9 fusion.206
  28.7 1.1 convolution_subtract_fusion.11
  30.1 0.8 fusion.205
  31.6 0.9 fusion.206
  33.1 1.1 convolution_subtract_fusion.11
  34.5 0.8 fusion.205
  35.9 0.9 fusion.206
  37.5 1.1 convolution_subtract_fusion.11
  38.8 0.8 fusion.205
  40.3 0.9 fusion.206
  41.8 1.1 convolution_subtract_fusion.11
  43.2 0.8 fusion.205
  44.7 0.9 fusion.206
  46.3 5.0 %collective-permute-start = (bf16[2,128,256]{2,1,0:T(8,128)(2,1)S(1)}, bf16[2,128,256]{2,1,0:T(8,128)(2,1)S(1)}, u32[]{:S(2)}, u32[]{:S(2)}) collective-permute-start(bf16[2,128,256]{2,1,0:T(8,128)(2,1)S(1)} %pad_maximum_fusion.6), channel_id=1, source_target_pairs={{0,4},{4,8},{8,12},{12,16},{16,20},{20,24},{24,28},{1,5},{5,9},{9,... | collective-permute-start | bytes 393224 | tf_op jit(solution)/shard_map/ppermute | solution.py:17
  51.3 5.5 %collective-permute-done = bf16[2,128,256]{2,1,0:T(8,128)(2,1)S(1)} collective-permute-done((bf16[2,128,256]{2,1,0:T(8,128)(2,1)S(1)}, bf16[2,128,256]{2,1,0:T(8,128)(2,1)S(1)}, u32[]{:S(2)}, u32[]{:S(2)}) %collective-permute-start) | collective-permute-done | bytes 131104 | tf_op jit(solution)/shard_map/ppermute | solution.py:17
  56.9 4.4 %collective-permute-start.1 = (bf16[2,128,256]{2,1,0:T(8,128)(2,1)S(1)}, bf16[2,128,256]{2,1,0:T(8,128)(2,1)S(1)}, u32[]{:S(2)}, u32[]{:S(2)}) collective-permute-start(bf16[2,128,256]{2,1,0:T(8,128)(2,1)S(1)} %collective-permute-done), channel_id=1, source_target_pairs={{0,4},{4,8},{8,12},{12,16},{16,20},{20,24},{24,28},{1,5},{5,9},{9,... | collective-permute-start | bytes 393224 | tf_op jit(solution)/shard_map/ppermute | solution.py:17
  61.2 5.4 %collective-permute-done.1 = bf16[2,128,256]{2,1,0:T(8,128)(2,1)S(1)} collective-permute-done((bf16[2,128,256]{2,1,0:T(8,128)(2,1)S(1)}, bf16[2,128,256]{2,1,0:T(8,128)(2,1)S(1)}, u32[]{:S(2)}, u32[]{:S(2)}) %collective-permute-start.1) | collective-permute-done | bytes 131104 | tf_op jit(solution)/shard_map/ppermute | solution.py:17
  66.9 6.0 %collective-permute-start.2 = (bf16[2,128,256]{2,1,0:T(8,128)(2,1)S(1)}, bf16[2,128,256]{2,1,0:T(8,128)(2,1)S(1)}, u32[]{:S(2)}, u32[]{:S(2)}) collective-permute-start(bf16[2,128,256]{2,1,0:T(8,128)(2,1)S(1)} %pad_maximum_fusion.7), channel_id=1, source_target_pairs={{0,8},{4,12},{8,16},{12,20},{16,24},{20,28},{1,9},{5,13},{9,17},{1... | collective-permute-start | bytes 393224 | tf_op jit(solution)/shard_map/ppermute | solution.py:17
  72.9 5.4 %collective-permute-done.2 = bf16[2,128,256]{2,1,0:T(8,128)(2,1)S(1)} collective-permute-done((bf16[2,128,256]{2,1,0:T(8,128)(2,1)S(1)}, bf16[2,128,256]{2,1,0:T(8,128)(2,1)S(1)}, u32[]{:S(2)}, u32[]{:S(2)}) %collective-permute-start.2) | collective-permute-done | bytes 131104 | tf_op jit(solution)/shard_map/ppermute | solution.py:17
  78.6 20.5 %collective-permute-start.3 = (bf16[2,128,128]{2,1,0:T(8,128)(2,1)S(1)}, bf16[2,128,128]{2,1,0:T(8,128)(2,1)S(1)}, u32[]{:S(2)}, u32[]{:S(2)}) collective-permute-start(bf16[2,128,128]{2,1,0:T(8,128)(2,1)S(1)} %fusion.128), channel_id=1, source_target_pairs={{0,16},{4,20},{8,24},{12,28},{1,17},{5,21},{9,25},{13,29},{2,18},{... | collective-permute-start | bytes 196616 | tf_op jit(solution)/shard_map/ppermute | solution.py:17
  99.3 2.9 collective-permute-done.3
  104.1 2.3 collective-permute-done.4
  106.9 11.1 %collective-permute-done.5 = bf16[96,2048]{1,0:T(8,128)(2,1)S(1)} collective-permute-done((bf16[96,2048]{1,0:T(8,128)(2,1)S(1)}, bf16[96,2048]{1,0:T(8,128)(2,1)S(1)}, u32[]{:S(2)}, u32[]{:S(2)}) %collective-permute-start.5) | collective-permute-done | bytes 393248 | tf_op jit(solution)/shard_map/ppermute | solution.py:50
  118.8 10.0 %collective-permute-done.6 = bf16[96,2048]{1,0:T(8,128)(2,1)S(1)} collective-permute-done((bf16[96,2048]{1,0:T(8,128)(2,1)S(1)}, bf16[96,2048]{1,0:T(8,128)(2,1)S(1)}, u32[]{:S(2)}, u32[]{:S(2)}) %collective-permute-start.6) | collective-permute-done | bytes 393248 | tf_op jit(solution)/shard_map/ppermute | solution.py:50
  129.6 1.8 collective-permute-done.7
  131.4 7.1 %fusion.47 = f32[384,1408]{1,0:T(8,128)} fusion(bf16[2048,1408]{1,0:T(8,128)(2,1)} %all-gather.4.cloned.1.call-done, bf16[192,2048]{1,0:T(8,128)(2,1)} %collective-permute-done.7, bf16[96,2048]{1,0:T(8,128)(2,1)} %copy-done.7, bf16[96,2048]{1,0:T(8,128)(2,1)} %copy-done.2), kind=kOutput, calls=%fused_computation.75 | convolution fusion | flops 2219311104 | bytes 9502720 | tf_op jit(solution)/shard_map/dot_general | solution.py:301
  138.5 67.4 %all-gather.6.cloned.1.call-done = bf16[2048,1408]{1,0:T(8,128)(2,1)} async-done(((bf16[256,1408]{1,0:T(8,128)(2,1)}), bf16[2048,1408]{1,0:T(8,128)(2,1)}) %all-gather.6.cloned.1.call-update) | async-done | bytes 5767184 | tf_op jit(solution)/shard_map/all_gather | solution.py:267
  206.0 7.4 %multiply_convert_fusion = bf16[384,1408]{1,0:T(8,128)(2,1)} fusion(f32[384,1408]{1,0:T(8,128)} %fusion.47, bf16[2048,1408]{1,0:T(8,128)(2,1)} %all-gather.6.cloned.1.call-done, bf16[192,2048]{1,0:T(8,128)(2,1)} %collective-permute-done.7, bf16[96,2048]{1,0:T(8,128)(2,1)} %copy-done.7, bf16[96,2048]{1,0:T(8,128)(2,1)} %copy-done.2), kind=kOutput, calls=%fused_computation.46 | convolution fusion | flops 2222555136 | bytes 10584064 | tf_op jit(solution)/shard_map/dot_general | solution.py:302
  213.4 86.0 %all-gather.8.cloned.1.call-done = bf16[1408,2048]{1,0:T(8,128)(2,1)} async-done(((bf16[1408,256]{1,0:T(8,128)(2,1)}), bf16[1408,2048]{1,0:T(8,128)(2,1)}) %all-gather.8.cloned.1.call-update) | async-done | bytes 5767184 | tf_op jit(solution)/shard_map/all_gather | solution.py:268
  299.4 4.3 %convolution_convert_fusion = bf16[192,2048]{1,0:T(8,128)(2,1)S(1)} fusion(bf16[1408,2048]{1,0:T(8,128)(2,1)} %all-gather.8.cloned.1.call-done, bf16[384,1408]{1,0:T(8,128)(2,1)} %multiply_convert_fusion), kind=kOutput, calls=%fused_computation.44 | convolution fusion | flops 1107689472 | bytes 7094272 | tf_op jit(solution)/shard_map/dot_general | solution.py:75
  303.8 2.3 collective-permute-done.8
  306.1 1.4 convert_add_fusion
  307.5 1.6 collective-permute-start.9
  309.1 9.6 %collective-permute-done.9 = bf16[96,2048]{1,0:T(8,128)(2,1)S(1)} collective-permute-done((bf16[96,2048]{1,0:T(8,128)(2,1)S(1)}, bf16[96,2048]{1,0:T(8,128)(2,1)S(1)}, u32[]{:S(2)}, u32[]{:S(2)}) %collective-permute-start.9) | collective-permute-done | bytes 393248 | tf_op jit(solution)/shard_map/ppermute | solution.py:50
  318.7 1.0 fusion.40
  (151 shorter events, 21.5 us)
Async XLA Ops:
  6.5 97.1 %copy-start = (bf16[256,2048]{1,0:T(8,128)(2,1)S(1)}, bf16[256,2048]{1,0:T(8,128)(2,1)}, u32[]{:S(2)}) copy-start(bf16[256,2048]{1,0:T(8,128)(2,1)} %param.27) | copy-start | bytes 3145732
  6.5 2.3 copy-start.16
  6.5 2.4 copy-start.12
  6.5 2.4 copy-start.11
  6.5 2.5 copy-start.3
  6.5 3.0 copy-start.13
  6.6 124.9 %all-gather.4.cloned.1.call-start = ((), (), s32[]{:S(2)}) async-start(), calls=%async_computation | async-start | bytes 6488064 | tf_op jit(solution)/shard_map/all_gather | solution.py:266
  7.3 198.7 %all-gather.6.cloned.1.call-start = ((), (), s32[]{:S(2)}) async-start(), calls=%async_computation.1 | async-start | bytes 6488064 | tf_op jit(solution)/shard_map/all_gather | solution.py:267
  8.0 291.3 %all-gather.8.cloned.1.call-start = ((), (), s32[]{:S(2)}) async-start(), calls=%async_computation.2 | async-start | bytes 6488064 | tf_op jit(solution)/shard_map/all_gather | solution.py:268
  14.4 2.3 copy-start.4
  14.9 2.1 copy-start.8
  46.2 52.9 %copy-start.5 = (f32[6,2,64,128]{3,2,0,1:T(8,128)S(1)}, f32[6,2,64,128]{3,2,0,1:T(8,128)}, u32[]{:S(2)}) copy-start(f32[6,2,64,128]{3,2,0,1:T(8,128)} %get-tuple-element.70) | copy-start | bytes 1179652
  46.2 56.2 %copy-start.6 = (f32[6,2,64,128]{3,2,0,1:T(8,128)S(1)}, f32[6,2,64,128]{3,2,0,1:T(8,128)}, u32[]{:S(2)}) copy-start(f32[6,2,64,128]{3,2,0,1:T(8,128)} %get-tuple-element.71) | copy-start | bytes 1179652
  46.3 10.6 %collective-permute-start = (bf16[2,128,256]{2,1,0:T(8,128)(2,1)S(1)}, bf16[2,128,256]{2,1,0:T(8,128)(2,1)S(1)}, u32[]{:S(2)}, u32[]{:S(2)}) collective-permute-start(bf16[2,128,256]{2,1,0:T(8,128)(2,1)S(1)} %pad_maximum_fusion.6), channel_id=1, source_target_pairs={{0,4},{4,8},{8,12},{12,16},{16,20},{20,24},{24,28},{1,5},{5,9},{9,... | collective-permute-start | bytes 393224 | tf_op jit(solution)/shard_map/ppermute | solution.py:17
  56.9 9.8 %collective-permute-start.1 = (bf16[2,128,256]{2,1,0:T(8,128)(2,1)S(1)}, bf16[2,128,256]{2,1,0:T(8,128)(2,1)S(1)}, u32[]{:S(2)}, u32[]{:S(2)}) collective-permute-start(bf16[2,128,256]{2,1,0:T(8,128)(2,1)S(1)} %collective-permute-done), channel_id=1, source_target_pairs={{0,4},{4,8},{8,12},{12,16},{16,20},{20,24},{24,28},{1,5},{5,9},{9,... | collective-permute-start | bytes 393224 | tf_op jit(solution)/shard_map/ppermute | solution.py:17
  66.8 36.3 %copy-start.14 = (f32[128]{0:T(128)S(1)}, f32[128]{0:T(128)}, u32[]{:S(2)}) copy-start(f32[128]{0:T(128)} %param.26) | copy-start | bytes 1540
  66.9 11.4 %collective-permute-start.2 = (bf16[2,128,256]{2,1,0:T(8,128)(2,1)S(1)}, bf16[2,128,256]{2,1,0:T(8,128)(2,1)S(1)}, u32[]{:S(2)}, u32[]{:S(2)}) collective-permute-start(bf16[2,128,256]{2,1,0:T(8,128)(2,1)S(1)} %pad_maximum_fusion.7), channel_id=1, source_target_pairs={{0,8},{4,12},{8,16},{12,20},{16,24},{20,28},{1,9},{5,13},{9,17},{1... | collective-permute-start | bytes 393224 | tf_op jit(solution)/shard_map/ppermute | solution.py:17
  78.6 24.8 %copy-start.9 = (bf16[384,256]{1,0:T(8,128)(2,1)S(1)}, bf16[384,256]{1,0:T(8,128)(2,1)}, u32[]{:S(2)}) copy-start(bf16[384,256]{1,0:T(8,128)(2,1)} %param.21) | copy-start | bytes 589828
  78.6 23.6 %collective-permute-start.3 = (bf16[2,128,128]{2,1,0:T(8,128)(2,1)S(1)}, bf16[2,128,128]{2,1,0:T(8,128)(2,1)S(1)}, u32[]{:S(2)}, u32[]{:S(2)}) collective-permute-start(bf16[2,128,128]{2,1,0:T(8,128)(2,1)S(1)} %fusion.128), channel_id=1, source_target_pairs={{0,16},{4,20},{8,24},{12,28},{1,17},{5,21},{9,25},{13,29},{2,18},{... | collective-permute-start | bytes 196616 | tf_op jit(solution)/shard_map/ppermute | solution.py:17
  104.0 14.0 %copy-start.1 = (bf16[96,2048]{1,0:T(8,128)(2,1)S(1)}, bf16[96,2048]{1,0:T(8,128)(2,1)}, u32[]{:S(2)}) copy-start(bf16[96,2048]{1,0:T(8,128)(2,1)} %param.17) | copy-start | bytes 1179652
  104.0 2.4 collective-permute-start.4
  106.3 11.9 %copy-start.10 = (f32[2048]{0:T(1024)S(1)}, f32[2048]{0:T(1024)}, u32[]{:S(2)}) copy-start(f32[2048]{0:T(1024)} %param.28) | copy-start | bytes 24580
  106.8 11.2 %collective-permute-start.5 = (bf16[96,2048]{1,0:T(8,128)(2,1)S(1)}, bf16[96,2048]{1,0:T(8,128)(2,1)S(1)}, u32[]{:S(2)}, u32[]{:S(2)}) collective-permute-start(bf16[96,2048]{1,0:T(8,128)(2,1)S(1)} %slice.148), channel_id=1, source_target_pairs={{0,2},{1,3},{2,0},{3,1},{4,6},{5,7},{6,4},{7,5},{8,10},{9,11},{10,... | collective-permute-start | bytes 1179656 | tf_op jit(solution)/shard_map/ppermute | solution.py:50
  118.5 10.4 %copy-start.2 = (bf16[96,2048]{1,0:T(8,128)(2,1)}, bf16[96,2048]{1,0:T(8,128)(2,1)S(1)}, u32[]{:S(2)}) copy-start(bf16[96,2048]{1,0:T(8,128)(2,1)S(1)} %multiply_convert_fusion.1) | copy-start | bytes 1179652
  118.5 10.4 %collective-permute-start.6 = (bf16[96,2048]{1,0:T(8,128)(2,1)S(1)}, bf16[96,2048]{1,0:T(8,128)(2,1)S(1)}, u32[]{:S(2)}, u32[]{:S(2)}) collective-permute-start(bf16[96,2048]{1,0:T(8,128)(2,1)S(1)} %multiply_convert_fusion.1), channel_id=1, source_target_pairs={{0,2},{1,3},{2,0},{3,1},{4,6},{5,7},{6,4},{7,5},{8,10},{9,11},{10,... | collective-permute-start | bytes 1179656 | tf_op jit(solution)/shard_map/ppermute | solution.py:50
  128.9 0.7 copy-start.7
  128.9 2.5 collective-permute-start.7
  299.4 6.7 %copy-start.15 = (bf16[1408,2048]{1,0:T(8,128)(2,1)S(1)}, bf16[1408,2048]{1,0:T(8,128)(2,1)}, u32[]{:S(2)}) copy-start(bf16[1408,2048]{1,0:T(8,128)(2,1)} %all-gather.8.cloned.1.call-done) | copy-start | bytes 17301508
  299.4 6.7 %copy-start.17 = (bf16[384,1408]{1,0:T(8,128)(2,1)S(1)}, bf16[384,1408]{1,0:T(8,128)(2,1)}, u32[]{:S(2)}) copy-start(bf16[384,1408]{1,0:T(8,128)(2,1)} %multiply_convert_fusion) | copy-start | bytes 3244036
  303.7 2.4 collective-permute-start.8
  307.5 11.2 %collective-permute-start.9 = (bf16[96,2048]{1,0:T(8,128)(2,1)S(1)}, bf16[96,2048]{1,0:T(8,128)(2,1)S(1)}, u32[]{:S(2)}, u32[]{:S(2)}) collective-permute-start(bf16[96,2048]{1,0:T(8,128)(2,1)S(1)} %slice.147), channel_id=1, source_target_pairs={{0,2},{1,3},{2,0},{3,1},{4,6},{5,7},{6,4},{7,5},{8,10},{9,11},{10,... | collective-permute-start | bytes 1179656 | tf_op jit(solution)/shard_map/ppermute | solution.py:50
Sparse Core Ops, SparseCore 0:
  9.5 99.7 all-gather.3
  111.5 94.4 all-gather.5
  208.0 91.2 all-gather.7

commit v2 on v1

--- a/solution.py
+++ b/solution.py
@@ -67,14 +67,61 @@
     return own
 
 
-def scatter_relative(left_rows, matrix):
+def takes_blocks(sp_size):
+    return sp_size % 2 == 0 and 4 <= sp_size <= 16
+
+
+def blocks_of_sp(shard, early_partner):
+    size = lax.axis_size("sp")
+    outer = size // 2
+
+    def along(by):
+        return lax.ppermute(shard, "sp", [(i, (i + 2 * by) % size) for i in range(size)])
+
+    turns = sorted(range(1, outer), key=lambda by: min(by, outer - by))
+    near = {0: shard} | {by: along(by) for by in turns}
+    far = {0: early_partner} | {by: swap(near[by], "sp", 1) for by in turns}
+    return [near[by] for by in range(outer)] + [far[by] for by in range(outer)]
+
+
+def block_sources():
+    size = lax.axis_size("sp")
+    outer = size // 2
+    me = lax.axis_index("sp")
+    return [
+        ((me // 2 + outer - by) % outer) * 2 + ((me % 2) ^ flip)
+        for flip in range(2)
+        for by in range(outer)
+    ]
+
+
+def absolute_columns(value):
+    size = lax.axis_size("sp")
+    outer = size // 2
+    width = value.shape[1] // size
+    me = lax.axis_index("sp")
+    pieces = []
+    for index in range(size):
+        by = (me // 2 + outer - index // 2) % outer
+        place = by + outer * ((me % 2) ^ (index % 2))
+        pieces.append(lax.dynamic_slice_in_dim(value, place * width, width, axis=1))
+    return jnp.concatenate(pieces, axis=1)
+
+
+def scatter_relative(left_rows, matrices):
+    def times(rows):
+        return jnp.concatenate(
+            [jnp.dot(rows, matrix, preferred_element_type=jnp.float32) for matrix in matrices],
+            axis=1,
+        )
+
     size = lax.axis_size("tp")
     if size == 1:
-        return jnp.dot(left_rows, matrix, preferred_element_type=jnp.float32)
+        return times(left_rows)
     half = left_rows.shape[0] // 2
-    leaving = jnp.dot(left_rows[half:], matrix, preferred_element_type=jnp.float32)
+    leaving = times(left_rows[half:])
     arrived = swap(leaving.astype(jnp.bfloat16), "tp", 1)
-    total = jnp.dot(left_rows[:half], matrix, preferred_element_type=jnp.float32)
+    total = times(left_rows[:half])
     total = total + arrived.astype(jnp.float32)
     bit = 2
     while bit < size:
@@ -264,8 +311,14 @@
     down_matrix,
 ):
     gate_whole = lax.all_gather(gate_matrix, "sp", axis=0, tiled=True)
-    up_whole = lax.all_gather(up_matrix, "sp", axis=0, tiled=True)
-    down_whole = lax.all_gather(down_matrix, "sp", axis=1, tiled=True)
+    sp_size = lax.axis_size("sp")
+    by_blocks = takes_blocks(sp_size)
+    if by_blocks:
+        up_partner = swap(up_matrix, "sp", 1)
+        down_partner = swap(down_matrix, "sp", 1)
+    else:
+        up_whole = lax.all_gather(up_matrix, "sp", axis=0, tiled=True)
+        down_whole = lax.all_gather(down_matrix, "sp", axis=1, tiled=True)
     block_outputs, decay_spans, matrix_product, running_state, _ = local_recurrence(
         query_projected,
         key_projected,
@@ -276,6 +329,12 @@
         head_decay_rate,
     )
     state_inflow = inflow_of_earlier(matrix_product, running_state)
+    if by_blocks:
+        state_inflow, up_matrix, down_matrix = lax.optimization_barrier(
+            (state_inflow, up_matrix, down_matrix)
+        )
+        up_blocks = blocks_of_sp(up_matrix, up_partner)
+        down_blocks = blocks_of_sp(down_matrix, down_partner)
     attention_output = block_outputs + jnp.einsum(
         "qwc,qcn->qwn", decay_spans, state_inflow, precision=PRECISION_FULL
     )
@@ -294,14 +353,33 @@
         ],
         axis=0,
     )
-    branch = scatter_relative(ordered, head_output_matrix)
+    branch = scatter_relative(ordered, [head_output_matrix])
     residual_own = stream.astype(jnp.float32) + branch
     normed_own = (rms_scale(residual_own) * feed_norm_gain).astype(jnp.bfloat16)
     whole_rows = gather_relative(normed_own)
     gate_total = jnp.dot(whole_rows, gate_whole, preferred_element_type=jnp.float32)
-    up_total = jnp.dot(whole_rows, up_whole, preferred_element_type=jnp.float32)
+    if by_blocks:
+        width = up_matrix.shape[0]
+        columns = [
+            lax.dynamic_slice_in_dim(whole_rows, source * width, width, axis=1)
+            for source in block_sources()
+        ]
+        half = sp_size // 2
+        up_total = sum(
+            jnp.dot(
+                jnp.concatenate(columns[part], axis=1),
+                jnp.concatenate(up_blocks[part], axis=0),
+                preferred_element_type=jnp.float32,
+            )
+            for part in (slice(None, half), slice(half, None))
+        )
+    else:
+        up_total = jnp.dot(whole_rows, up_whole, preferred_element_type=jnp.float32)
     hidden = (jax.nn.silu(gate_total) * up_total).astype(jnp.bfloat16)
-    ffn_own = scatter_relative(hidden, down_whole)
+    if by_blocks:
+        ffn_own = absolute_columns(scatter_relative(hidden, down_blocks))
+    else:
+        ffn_own = scatter_relative(hidden, [down_whole])
     return (residual_own + ffn_own).astype(jnp.bfloat16)
 
 
@@ -323,6 +401,7 @@
         P("sp", "tp"),
         P("tp", "sp"),
     )
+
     return jax.shard_map(
         body, mesh=mesh, in_specs=placed, out_specs=P(("sp", "tp"), None), check_vma=False
     )

time: 327 us -> 355 us (1.086)
  starting transfers between devices: 38.3 us -> 61 us
  waiting for transfers between devices: 212 us -> 199 us
  matrix products: 55.6 us -> 63.2 us
  other arithmetic: 3.82 us -> 9.79 us
  local copies, waits for them, and re-layouts: 2.49 us -> 6.29 us
    all_gather x2 -> x0, waiting for transfers between devices: 153 us -> none  [the longest x1 86 us: body(): down_whole = lax.all_gather(down_matrix, 'sp', axis=1, tiled=True)]
    ppermute x0 -> x6, waiting for transfers between devices: none -> 75.4 us  [along(): lax.ppermute(shard, 'sp', [(i, (i + 2 * by) % size) for i in range(size)])]
    ppermute x6 -> x14, waiting for transfers between devices: 37.2 us -> 103 us  [swap(): return lax.ppermute(value, axis, [(i, i ^ bit) for i in range(size)])]
    ppermute x0 -> x6, starting transfers between devices: none -> 11.9 us  [along(): lax.ppermute(shard, 'sp', [(i, (i + 2 * by) % size) for i in range(size)])]
    ppermute x6 -> x14, starting transfers between devices: 2.22 us -> 13 us  [swap(): return lax.ppermute(value, axis, [(i, i ^ bit) for i in range(size)])]
    dot_general x5 -> x20, matrix products: 13.9 us -> 22.7 us  [the longest x18 14.9 us: times(): jnp.dot(rows, matrix, preferred_element_type=jnp.float32)]
  transfers between devices with their start and end apart: 13 -> 25, of which waited for: 12 -> 17; matrix products, arithmetic and copies ran while one was open for 17% -> 21% of each run, Pallas kernels for 0% -> 0%
where the time goes in v2:
time: 355 us; the launch traced here: 354 us
  waiting for transfers between devices  199 us (56%)
  matrix products  63.2 us (18%)
  starting transfers between devices  61 us (17%)
  between operations  14.3 us (4%)
  other arithmetic  9.79 us (3%)
  local copies, waits for them, and re-layouts  6.29 us (2%)
    ppermute x14, waiting for transfers between devices, swap(): return lax.ppermute(value, axis, [(i, i ^ bit) for i in range(size)])  103 us
    ppermute x6, waiting for transfers between devices, along(): lax.ppermute(shard, 'sp', [(i, (i + 2 * by) % size) for i in range(size)])  75.4 us
    ppermute x4, starting transfers between devices, from_behind(): return lax.ppermute(value, axis, pairs)  36 us
    ppermute x4, waiting for transfers between devices, from_behind(): return lax.ppermute(value, axis, pairs)  19.5 us
    dot_general x18, matrix products, times(): jnp.dot(rows, matrix, preferred_element_type=jnp.float32)  14.9 us
    ppermute x14, starting transfers between devices, swap(): return lax.ppermute(value, axis, [(i, i ^ bit) for i in range(size)])  13 us
    ppermute x6, starting transfers between devices, along(): lax.ppermute(shard, 'sp', [(i, (i + 2 * by) % size) for i in range(size)])  11.9 us
    dot_general x2, matrix products, body(): jnp.dot(jnp.concatenate(columns[part], axis=1), jnp.concatenate(up_blocks...  7.86 us
  transfers between devices with their start and end apart: 25, of which 17 were waited for; matrix products, arithmetic and copies ran while one was open for 21% of the time, Pallas kernels for 0%

profile of v2, /device:TPU:0, one launch (start us, length us, event | category | flops | bytes accessed | tf_op | source)
XLA Modules:
  0.0 353.8 jit_solution(5316443480661976863)
XLA Ops:
  8.9 1.1 fusion.96
  10.0 1.1 fusion.94
  21.6 26.3 %while.17 = (s32[]{:T(128)}, f32[2,128,128]{2,1,0:T(8,128)S(1)}, f32[2,128,128]{2,1,0:T(8,128)S(1)}, f32[6,2,64,128]{3,2,0,1:T(8,128)}, f32[6,2,64,128]{3,2,0,1:...) while((s32[]{:T(128)}, f32[2,128,128]{2,1,0:T(8,128)S(1)}, ...), condition=%wide.region_4.5_spmd.clone, body=%wide.region_3.4_spmd.clone.sunk | while | flops 201605120 | bytes 2758829 | solution.py:280
  48.0 5.0 %collective-permute-start = (bf16[2,128,256]{2,1,0:T(8,128)(2,1)S(1)}, bf16[2,128,256]{2,1,0:T(8,128)(2,1)S(1)}, u32[]{:S(2)}, u32[]{:S(2)}) collective-permute-start(bf16[2,128,256]{2,1,0:T(8,128)(2,1)S(1)} %pad_maximum_fusion.2), channel_id=1, source_target_pairs={{0,4},{4,8},{8,12},{12,16},{16,20},{20,24},{24,28},{1,5},{5,9},{9,... | collective-permute-start | bytes 393224 | tf_op jit(solution)/shard_map/ppermute | solution.py:17
  53.1 6.2 %collective-permute-done = bf16[2,128,256]{2,1,0:T(8,128)(2,1)S(1)} collective-permute-done((bf16[2,128,256]{2,1,0:T(8,128)(2,1)S(1)}, bf16[2,128,256]{2,1,0:T(8,128)(2,1)S(1)}, u32[]{:S(2)}, u32[]{:S(2)}) %collective-permute-start) | collective-permute-done | bytes 131104 | tf_op jit(solution)/shard_map/ppermute | solution.py:17
  59.3 4.4 %collective-permute-start.1 = (bf16[2,128,256]{2,1,0:T(8,128)(2,1)S(1)}, bf16[2,128,256]{2,1,0:T(8,128)(2,1)S(1)}, u32[]{:S(2)}, u32[]{:S(2)}) collective-permute-start(bf16[2,128,256]{2,1,0:T(8,128)(2,1)S(1)} %collective-permute-done), channel_id=1, source_target_pairs={{0,4},{4,8},{8,12},{12,16},{16,20},{20,24},{24,28},{1,5},{5,9},{9,... | collective-permute-start | bytes 393224 | tf_op jit(solution)/shard_map/ppermute | solution.py:17
  63.7 6.0 %collective-permute-done.1 = bf16[2,128,256]{2,1,0:T(8,128)(2,1)S(1)} collective-permute-done((bf16[2,128,256]{2,1,0:T(8,128)(2,1)S(1)}, bf16[2,128,256]{2,1,0:T(8,128)(2,1)S(1)}, u32[]{:S(2)}, u32[]{:S(2)}) %collective-permute-start.1) | collective-permute-done | bytes 131104 | tf_op jit(solution)/shard_map/ppermute | solution.py:17
  70.0 6.4 %collective-permute-start.2 = (bf16[2,128,256]{2,1,0:T(8,128)(2,1)S(1)}, bf16[2,128,256]{2,1,0:T(8,128)(2,1)S(1)}, u32[]{:S(2)}, u32[]{:S(2)}) collective-permute-start(bf16[2,128,256]{2,1,0:T(8,128)(2,1)S(1)} %pad_maximum_fusion.3), channel_id=1, source_target_pairs={{0,8},{4,12},{8,16},{12,20},{16,24},{20,28},{1,9},{5,13},{9,17},{1... | collective-permute-start | bytes 393224 | tf_op jit(solution)/shard_map/ppermute | solution.py:17
  76.4 5.8 %collective-permute-done.2 = bf16[2,128,256]{2,1,0:T(8,128)(2,1)S(1)} collective-permute-done((bf16[2,128,256]{2,1,0:T(8,128)(2,1)S(1)}, bf16[2,128,256]{2,1,0:T(8,128)(2,1)S(1)}, u32[]{:S(2)}, u32[]{:S(2)}) %collective-permute-start.2) | collective-permute-done | bytes 131104 | tf_op jit(solution)/shard_map/ppermute | solution.py:17
  82.5 20.2 %collective-permute-start.3 = (bf16[2,128,128]{2,1,0:T(8,128)(2,1)S(1)}, bf16[2,128,128]{2,1,0:T(8,128)(2,1)S(1)}, u32[]{:S(2)}, u32[]{:S(2)}) collective-permute-start(bf16[2,128,128]{2,1,0:T(8,128)(2,1)S(1)} %fusion.176), channel_id=1, source_target_pairs={{0,16},{4,20},{8,24},{12,28},{1,17},{5,21},{9,25},{13,29},{2,18},{... | collective-permute-start | bytes 196616 | tf_op jit(solution)/shard_map/ppermute | solution.py:17
  102.9 1.5 collective-permute-done.3
  106.2 2.3 collective-permute-done.4
  109.9 10.2 %collective-permute-done.5 = bf16[96,2048]{1,0:T(8,128)(2,1)S(1)} collective-permute-done((bf16[96,2048]{1,0:T(8,128)(2,1)S(1)}, bf16[96,2048]{1,0:T(8,128)(2,1)S(1)}, u32[]{:S(2)}, u32[]{:S(2)}) %collective-permute-start.5) | collective-permute-done | bytes 393248 | tf_op jit(solution)/shard_map/ppermute | solution.py:50
  121.9 9.4 %collective-permute-done.6 = bf16[96,2048]{1,0:T(8,128)(2,1)S(1)} collective-permute-done((bf16[96,2048]{1,0:T(8,128)(2,1)S(1)}, bf16[96,2048]{1,0:T(8,128)(2,1)S(1)}, u32[]{:S(2)}, u32[]{:S(2)}) %collective-permute-start.6) | collective-permute-done | bytes 393248 | tf_op jit(solution)/shard_map/ppermute | solution.py:50
  132.2 2.6 collective-permute-start.10
  134.8 2.9 collective-permute-start.9
  138.7 1.5 collective-permute-start.15
  140.2 1.3 pad_maximum_fusion
  142.6 8.5 %collective-permute-done.11 = bf16[256,1408]{1,0:T(8,128)(2,1)} collective-permute-done((bf16[256,1408]{1,0:T(8,128)(2,1)}, bf16[256,1408]{1,0:T(8,128)(2,1)}, u32[]{:S(2)}, u32[]{:S(2)}) %collective-permute-start.11) | collective-permute-done | bytes 720928 | tf_op jit(solution)/shard_map/ppermute | solution.py:50
  151.0 3.4 collective-permute-start.16
  154.4 1.6 collective-permute-start.17
  156.0 14.0 %collective-permute-done.8 = bf16[256,1408]{1,0:T(8,128)(2,1)} collective-permute-done((bf16[256,1408]{1,0:T(8,128)(2,1)}, bf16[256,1408]{1,0:T(8,128)(2,1)}, u32[]{:S(2)}, u32[]{:S(2)}) %collective-permute-start.8) | collective-permute-done | bytes 720928 | tf_op jit(solution)/shard_map/ppermute | solution.py:79
  170.0 2.0 collective-permute-start.12
  172.0 58.3 %collective-permute-done.9 = bf16[256,1408]{1,0:T(8,128)(2,1)} collective-permute-done((bf16[256,1408]{1,0:T(8,128)(2,1)}, bf16[256,1408]{1,0:T(8,128)(2,1)}, u32[]{:S(2)}, u32[]{:S(2)}) %collective-permute-start.9) | collective-permute-done | bytes 720928 | tf_op jit(solution)/shard_map/ppermute | solution.py:79
  230.3 2.0 collective-permute-start.13
  232.3 4.5 %fusion.39 = f32[384,1408]{1,0:T(8,128)} fusion(bf16[256,1408]{1,0:T(8,128)(2,1)} %collective-permute-done.10, bf16[256,1408]{1,0:T(8,128)(2,1)} %collective-permute-done.9, bf16[256,1408]{1,0:T(8,128)(2,1)} %collective-permute-done.8, bf16[256,1408]{1,0:T(8,128)(2,1)} %param.30, bf16[384,256]{1,0:T(8,128)(2,1)S(1)} %get-tuple-element.173, ...), kind=kOutput, calls=%fused_computation.46 | convolution fusion | flops 1121976320 | bytes 5832704 | tf_op jit(solution)/shard_map/dot_general | solution.py:369
  236.8 5.7 %fusion.177 = f32[384,1408]{1,0:T(8,128)S(1)} fusion(bf16[2048,1408]{1,0:T(8,128)(2,1)} %all-gather.2.cloned.1.call-done, bf16[192,2048]{1,0:T(8,128)(2,1)} %copy-done.7, bf16[96,2048]{1,0:T(8,128)(2,1)} %copy-done.5, bf16[96,2048]{1,0:T(8,128)(2,1)S(1)} %multiply_convert_fusion), kind=kOutput, calls=%fused_computation.300 | convolution fusion | flops 2219311104 | bytes 9502720 | tf_op jit(solution)/shard_map/dot_general | solution.py:360
  242.6 3.1 collective-permute-done.16
  245.7 2.0 collective-permute-start.18
  247.7 2.0 collective-permute-start.20
  249.7 1.8 collective-permute-start.21
  251.6 13.5 %collective-permute-done.14 = bf16[256,1408]{1,0:T(8,128)(2,1)} collective-permute-done((bf16[256,1408]{1,0:T(8,128)(2,1)}, bf16[256,1408]{1,0:T(8,128)(2,1)}, u32[]{:S(2)}, u32[]{:S(2)}) %collective-permute-start.14) | collective-permute-done | bytes 720928 | tf_op jit(solution)/shard_map/ppermute | solution.py:50
  265.1 3.3 fusion.54
  268.4 1.4 fusion.58
  269.9 1.4 fusion.59
  271.3 1.4 fusion.60
  272.8 1.4 fusion.61
  274.2 6.2 %collective-permute-done.18 = bf16[1408,256]{1,0:T(8,128)(2,1)S(1)} collective-permute-done((bf16[1408,256]{1,0:T(8,128)(2,1)}, bf16[1408,256]{1,0:T(8,128)(2,1)S(1)}, u32[]{:S(2)}, u32[]{:S(2)}) %collective-permute-start.18) | collective-permute-done | bytes 720928 | tf_op jit(solution)/shard_map/ppermute | solution.py:50
  280.7 15.1 %collective-permute-done.19 = bf16[1408,256]{1,0:T(8,128)(2,1)S(1)} collective-permute-done((bf16[1408,256]{1,0:T(8,128)(2,1)}, bf16[1408,256]{1,0:T(8,128)(2,1)S(1)}, u32[]{:S(2)}, u32[]{:S(2)}) %collective-permute-start.19) | collective-permute-done | bytes 720928 | tf_op jit(solution)/shard_map/ppermute | solution.py:50
  296.1 15.1 %collective-permute-done.20 = bf16[1408,256]{1,0:T(8,128)(2,1)S(1)} collective-permute-done((bf16[1408,256]{1,0:T(8,128)(2,1)}, bf16[1408,256]{1,0:T(8,128)(2,1)S(1)}, u32[]{:S(2)}, u32[]{:S(2)}) %collective-permute-start.20) | collective-permute-done | bytes 720928 | tf_op jit(solution)/shard_map/ppermute | solution.py:50
  311.6 1.4 convolution_dynamic-update-slice_fusion.7
  313.1 12.2 %collective-permute-done.21 = bf16[1408,256]{1,0:T(8,128)(2,1)S(1)} collective-permute-done((bf16[1408,256]{1,0:T(8,128)(2,1)}, bf16[1408,256]{1,0:T(8,128)(2,1)S(1)}, u32[]{:S(2)}, u32[]{:S(2)}) %collective-permute-start.21) | collective-permute-done | bytes 720928 | tf_op jit(solution)/shard_map/ppermute | solution.py:50
  325.7 1.4 convolution_dynamic-update-slice_fusion.6
  327.1 1.4 convolution_dynamic-update-slice_fusion.5
  328.6 1.4 convolution_dynamic-update-slice_fusion.4
  331.6 1.2 copy-done.1
  333.8 10.7 %collective-permute-done.23 = bf16[96,2048]{1,0:T(8,128)(2,1)} collective-permute-done((bf16[96,2048]{1,0:T(8,128)(2,1)S(1)}, bf16[96,2048]{1,0:T(8,128)(2,1)}, u32[]{:S(2)}, u32[]{:S(2)}) %collective-permute-start.23) | collective-permute-done | bytes 393248 | tf_op jit(solution)/shard_map/ppermute | solution.py:50
  344.5 1.3 slice_add_fusion
  (204 shorter events, 52.1 us)
Async XLA Ops:
  6.5 99.2 %copy-start = (bf16[256,2048]{1,0:T(8,128)(2,1)S(1)}, bf16[256,2048]{1,0:T(8,128)(2,1)}, u32[]{:S(2)}) copy-start(bf16[256,2048]{1,0:T(8,128)(2,1)} %param.27) | copy-start | bytes 3145732
  6.5 4.6 %copy-start.17 = (bf16[2,384]{1,0:T(2,128)(2,1)S(1)}, bf16[2,384]{1,0:T(2,128)(2,1)}, u32[]{:S(2)}) copy-start(bf16[2,384]{1,0:T(2,128)(2,1)} %param.22) | copy-start | bytes 4612
  6.5 230.3 %all-gather.2.cloned.1.call-start = ((), (), s32[]{:S(2)}) async-start(), calls=%async_computation | async-start | bytes 6488064 | tf_op jit(solution)/shard_map/all_gather | solution.py:313
  16.5 1.7 copy-start.6
  17.1 1.5 copy-start.14
  47.9 54.8 %copy-start.8 = (f32[6,2,64,128]{3,2,0,1:T(8,128)S(1)}, f32[6,2,64,128]{3,2,0,1:T(8,128)}, u32[]{:S(2)}) copy-start(f32[6,2,64,128]{3,2,0,1:T(8,128)} %get-tuple-element.73) | copy-start | bytes 1179652
  48.0 11.3 %collective-permute-start = (bf16[2,128,256]{2,1,0:T(8,128)(2,1)S(1)}, bf16[2,128,256]{2,1,0:T(8,128)(2,1)S(1)}, u32[]{:S(2)}, u32[]{:S(2)}) collective-permute-start(bf16[2,128,256]{2,1,0:T(8,128)(2,1)S(1)} %pad_maximum_fusion.2), channel_id=1, source_target_pairs={{0,4},{4,8},{8,12},{12,16},{16,20},{20,24},{24,28},{1,5},{5,9},{9,... | collective-permute-start | bytes 393224 | tf_op jit(solution)/shard_map/ppermute | solution.py:17
  59.3 10.4 %collective-permute-start.1 = (bf16[2,128,256]{2,1,0:T(8,128)(2,1)S(1)}, bf16[2,128,256]{2,1,0:T(8,128)(2,1)S(1)}, u32[]{:S(2)}, u32[]{:S(2)}) collective-permute-start(bf16[2,128,256]{2,1,0:T(8,128)(2,1)S(1)} %collective-permute-done), channel_id=1, source_target_pairs={{0,4},{4,8},{8,12},{12,16},{16,20},{20,24},{24,28},{1,5},{5,9},{9,... | collective-permute-start | bytes 393224 | tf_op jit(solution)/shard_map/ppermute | solution.py:17
  69.9 34.7 %copy-start.9 = (f32[6,2,64,128]{3,2,0,1:T(8,128)S(1)}, f32[6,2,64,128]{3,2,0,1:T(8,128)}, u32[]{:S(2)}) copy-start(f32[6,2,64,128]{3,2,0,1:T(8,128)} %get-tuple-element.74) | copy-start | bytes 1179652
  70.0 12.2 %collective-permute-start.2 = (bf16[2,128,256]{2,1,0:T(8,128)(2,1)S(1)}, bf16[2,128,256]{2,1,0:T(8,128)(2,1)S(1)}, u32[]{:S(2)}, u32[]{:S(2)}) collective-permute-start(bf16[2,128,256]{2,1,0:T(8,128)(2,1)S(1)} %pad_maximum_fusion.3), channel_id=1, source_target_pairs={{0,8},{4,12},{8,16},{12,20},{16,24},{20,28},{1,9},{5,13},{9,17},{1... | collective-permute-start | bytes 393224 | tf_op jit(solution)/shard_map/ppermute | solution.py:17
  82.4 22.9 %copy-start.18 = (f32[128]{0:T(128)S(1)}, f32[128]{0:T(128)}, u32[]{:S(2)}) copy-start(f32[128]{0:T(128)} %param.26) | copy-start | bytes 1540
  82.5 21.9 %collective-permute-start.3 = (bf16[2,128,128]{2,1,0:T(8,128)(2,1)S(1)}, bf16[2,128,128]{2,1,0:T(8,128)(2,1)S(1)}, u32[]{:S(2)}, u32[]{:S(2)}) collective-permute-start(bf16[2,128,128]{2,1,0:T(8,128)(2,1)S(1)} %fusion.176), channel_id=1, source_target_pairs={{0,16},{4,20},{8,24},{12,28},{1,17},{5,21},{9,25},{13,29},{2,18},{... | collective-permute-start | bytes 196616 | tf_op jit(solution)/shard_map/ppermute | solution.py:17
  104.6 1.0 copy-start.15
  106.2 2.4 collective-permute-start.4
  108.5 11.7 %copy-start.2 = (bf16[96,2048]{1,0:T(8,128)(2,1)S(1)}, bf16[96,2048]{1,0:T(8,128)(2,1)}, u32[]{:S(2)}) copy-start(bf16[96,2048]{1,0:T(8,128)(2,1)} %param.17) | copy-start | bytes 1179652
  108.9 11.6 %copy-start.16 = (f32[2048]{0:T(1024)S(1)}, f32[2048]{0:T(1024)}, u32[]{:S(2)}) copy-start(f32[2048]{0:T(1024)} %param.28) | copy-start | bytes 24580
  109.0 11.2 %collective-permute-start.5 = (bf16[96,2048]{1,0:T(8,128)(2,1)S(1)}, bf16[96,2048]{1,0:T(8,128)(2,1)S(1)}, u32[]{:S(2)}, u32[]{:S(2)}) collective-permute-start(bf16[96,2048]{1,0:T(8,128)(2,1)S(1)} %slice.170), channel_id=1, source_target_pairs={{0,2},{1,3},{2,0},{3,1},{4,6},{5,7},{6,4},{7,5},{8,10},{9,11},{10,... | collective-permute-start | bytes 1179656 | tf_op jit(solution)/shard_map/ppermute | solution.py:50
  120.2 0.8 copy-start.3
  121.0 10.3 %collective-permute-start.6 = (bf16[96,2048]{1,0:T(8,128)(2,1)S(1)}, bf16[96,2048]{1,0:T(8,128)(2,1)S(1)}, u32[]{:S(2)}, u32[]{:S(2)}) collective-permute-start(bf16[96,2048]{1,0:T(8,128)(2,1)S(1)} %multiply_convert_fusion), channel_id=1, source_target_pairs={{0,2},{1,3},{2,0},{3,1},{4,6},{5,7},{6,4},{7,5},{8,10},{9,11},{10,... | collective-permute-start | bytes 1179656 | tf_op jit(solution)/shard_map/ppermute | solution.py:50
  131.3 0.7 copy-start.5
  132.1 5.6 %collective-permute-start.7 = (bf16[192,2048]{1,0:T(8,128)(2,1)S(1)}, bf16[192,2048]{1,0:T(8,128)(2,1)S(1)}, u32[]{:S(2)}, u32[]{:S(2)}) collective-permute-start(bf16[192,2048]{1,0:T(8,128)(2,1)S(1)} %pad_maximum_fusion.1), channel_id=1, source_target_pairs={{0,1},{1,0},{2,3},{3,2},{4,5},{5,4},{6,7},{7,6},{8,9},{9,8},{10,11... | collective-permute-start | bytes 2359304 | tf_op jit(solution)/shard_map/ppermute | solution.py:50
  132.2 18.9 %collective-permute-start.11 = (bf16[256,1408]{1,0:T(8,128)(2,1)}, bf16[256,1408]{1,0:T(8,128)(2,1)}, u32[]{:S(2)}, u32[]{:S(2)}) collective-permute-start(bf16[256,1408]{1,0:T(8,128)(2,1)} %param.30), channel_id=1, source_target_pairs={{0,4},{4,0},{8,12},{12,8},{16,20},{20,16},{24,28},{28,24},{1,5},{5... | collective-permute-start | bytes 2162696 | tf_op jit(solution)/shard_map/ppermute | solution.py:50
  132.2 22.1 %collective-permute-start.10 = (bf16[256,1408]{1,0:T(8,128)(2,1)}, bf16[256,1408]{1,0:T(8,128)(2,1)}, u32[]{:S(2)}, u32[]{:S(2)}) collective-permute-start(bf16[256,1408]{1,0:T(8,128)(2,1)} %param.30), channel_id=1, source_target_pairs={{0,24},{4,28},{8,0},{12,4},{16,8},{20,12},{24,16},{28,20},{1,25},{... | collective-permute-start | bytes 2162696 | tf_op jit(solution)/shard_map/ppermute | solution.py:79
  134.8 35.2 %collective-permute-start.8 = (bf16[256,1408]{1,0:T(8,128)(2,1)}, bf16[256,1408]{1,0:T(8,128)(2,1)}, u32[]{:S(2)}, u32[]{:S(2)}) collective-permute-start(bf16[256,1408]{1,0:T(8,128)(2,1)} %param.30), channel_id=1, source_target_pairs={{0,8},{4,12},{8,16},{12,20},{16,24},{20,28},{24,0},{28,4},{1,9},{5... | collective-permute-start | bytes 2162696 | tf_op jit(solution)/shard_map/ppermute | solution.py:79
  134.8 95.5 %collective-permute-start.9 = (bf16[256,1408]{1,0:T(8,128)(2,1)}, bf16[256,1408]{1,0:T(8,128)(2,1)}, u32[]{:S(2)}, u32[]{:S(2)}) collective-permute-start(bf16[256,1408]{1,0:T(8,128)(2,1)} %param.30), channel_id=1, source_target_pairs={{0,16},{4,20},{8,24},{12,28},{16,0},{20,4},{24,8},{28,12},{1,17},{... | collective-permute-start | bytes 2162696 | tf_op jit(solution)/shard_map/ppermute | solution.py:79
  137.7 1.0 copy-start.7
  138.7 93.6 %collective-permute-start.15 = (bf16[1408,256]{1,0:T(8,128)(2,1)}, bf16[1408,256]{1,0:T(8,128)(2,1)}, u32[]{:S(2)}, u32[]{:S(2)}) collective-permute-start(bf16[1408,256]{1,0:T(8,128)(2,1)} %param.31), channel_id=1, source_target_pairs={{0,8},{4,12},{8,16},{12,20},{16,24},{20,28},{24,0},{28,4},{1,9},{5... | collective-permute-start | bytes 2162696 | tf_op jit(solution)/shard_map/ppermute | solution.py:79
  151.0 94.7 %collective-permute-start.16 = (bf16[1408,256]{1,0:T(8,128)(2,1)}, bf16[1408,256]{1,0:T(8,128)(2,1)}, u32[]{:S(2)}, u32[]{:S(2)}) collective-permute-start(bf16[1408,256]{1,0:T(8,128)(2,1)} %param.31), channel_id=1, source_target_pairs={{0,16},{4,20},{8,24},{12,28},{16,0},{20,4},{24,8},{28,12},{1,17},{... | collective-permute-start | bytes 2162696 | tf_op jit(solution)/shard_map/ppermute | solution.py:79
  154.4 93.3 %collective-permute-start.17 = (bf16[1408,256]{1,0:T(8,128)(2,1)}, bf16[1408,256]{1,0:T(8,128)(2,1)}, u32[]{:S(2)}, u32[]{:S(2)}) collective-permute-start(bf16[1408,256]{1,0:T(8,128)(2,1)} %param.31), channel_id=1, source_target_pairs={{0,24},{4,28},{8,0},{12,4},{16,8},{20,12},{24,16},{28,20},{1,25},{... | collective-permute-start | bytes 2162696 | tf_op jit(solution)/shard_map/ppermute | solution.py:79
  170.0 77.7 %collective-permute-start.12 = (bf16[256,1408]{1,0:T(8,128)(2,1)}, bf16[256,1408]{1,0:T(8,128)(2,1)}, u32[]{:S(2)}, u32[]{:S(2)}) collective-permute-start(bf16[256,1408]{1,0:T(8,128)(2,1)} %collective-permute-done.8), channel_id=1, source_target_pairs={{0,4},{4,0},{8,12},{12,8},{16,20},{20,16},{24,28},{28,24},{1,5},{5... | collective-permute-start | bytes 2162696 | tf_op jit(solution)/shard_map/ppermute | solution.py:50
  230.3 19.5 %collective-permute-start.13 = (bf16[256,1408]{1,0:T(8,128)(2,1)}, bf16[256,1408]{1,0:T(8,128)(2,1)}, u32[]{:S(2)}, u32[]{:S(2)}) collective-permute-start(bf16[256,1408]{1,0:T(8,128)(2,1)} %collective-permute-done.9), channel_id=1, source_target_pairs={{0,4},{4,0},{8,12},{12,8},{16,20},{20,16},{24,28},{28,24},{1,5},{5... | collective-permute-start | bytes 2162696 | tf_op jit(solution)/shard_map/ppermute | solution.py:50
  232.2 32.8 %collective-permute-start.14 = (bf16[256,1408]{1,0:T(8,128)(2,1)}, bf16[256,1408]{1,0:T(8,128)(2,1)}, u32[]{:S(2)}, u32[]{:S(2)}) collective-permute-start(bf16[256,1408]{1,0:T(8,128)(2,1)} %collective-permute-done.10), channel_id=1, source_target_pairs={{0,4},{4,0},{8,12},{12,8},{16,20},{20,16},{24,28},{28,24},{1,5},{5... | collective-permute-start | bytes 2162696 | tf_op jit(solution)/shard_map/ppermute | solution.py:50
  236.8 28.2 %copy-start.10 = (bf16[384,256]{1,0:T(8,128)(2,1)S(1)}, bf16[384,256]{1,0:T(8,128)(2,1)}, u32[]{:S(2)}) copy-start(bf16[384,256]{1,0:T(8,128)(2,1)} %get-tuple-element.170) | copy-start | bytes 589828
  236.8 28.2 %copy-start.11 = (bf16[384,256]{1,0:T(8,128)(2,1)S(1)}, bf16[384,256]{1,0:T(8,128)(2,1)}, u32[]{:S(2)}) copy-start(bf16[384,256]{1,0:T(8,128)(2,1)} %get-tuple-element.171) | copy-start | bytes 589828
  236.8 28.2 %copy-start.12 = (bf16[384,256]{1,0:T(8,128)(2,1)S(1)}, bf16[384,256]{1,0:T(8,128)(2,1)}, u32[]{:S(2)}) copy-start(bf16[384,256]{1,0:T(8,128)(2,1)} %get-tuple-element.172) | copy-start | bytes 589828
  236.8 28.2 %copy-start.13 = (bf16[384,256]{1,0:T(8,128)(2,1)S(1)}, bf16[384,256]{1,0:T(8,128)(2,1)}, u32[]{:S(2)}) copy-start(bf16[384,256]{1,0:T(8,128)(2,1)} %get-tuple-element.177) | copy-start | bytes 589828
  236.8 28.2 %copy-start.19 = (f32[384,1408]{1,0:T(8,128)S(1)}, f32[384,1408]{1,0:T(8,128)}, u32[]{:S(2)}) copy-start(f32[384,1408]{1,0:T(8,128)} %fusion.39) | copy-start | bytes 6488068
  245.7 34.7 %collective-permute-start.18 = (bf16[1408,256]{1,0:T(8,128)(2,1)}, bf16[1408,256]{1,0:T(8,128)(2,1)S(1)}, u32[]{:S(2)}, u32[]{:S(2)}) collective-permute-start(bf16[1408,256]{1,0:T(8,128)(2,1)} %param.31), channel_id=1, source_target_pairs={{0,4},{4,0},{8,12},{12,8},{16,20},{20,16},{24,28},{28,24},{1,5},{5... | collective-permute-start | bytes 2162696 | tf_op jit(solution)/shard_map/ppermute | solution.py:50
  247.7 48.1 %collective-permute-start.19 = (bf16[1408,256]{1,0:T(8,128)(2,1)}, bf16[1408,256]{1,0:T(8,128)(2,1)S(1)}, u32[]{:S(2)}, u32[]{:S(2)}) collective-permute-start(bf16[1408,256]{1,0:T(8,128)(2,1)} %collective-permute-done.15), channel_id=1, source_target_pairs={{0,4},{4,0},{8,12},{12,8},{16,20},{20,16},{24,28},{28,24},{1,5},{5... | collective-permute-start | bytes 2162696 | tf_op jit(solution)/shard_map/ppermute | solution.py:50
  247.7 63.5 %collective-permute-start.20 = (bf16[1408,256]{1,0:T(8,128)(2,1)}, bf16[1408,256]{1,0:T(8,128)(2,1)S(1)}, u32[]{:S(2)}, u32[]{:S(2)}) collective-permute-start(bf16[1408,256]{1,0:T(8,128)(2,1)} %collective-permute-done.16), channel_id=1, source_target_pairs={{0,4},{4,0},{8,12},{12,8},{16,20},{20,16},{24,28},{28,24},{1,5},{5... | collective-permute-start | bytes 2162696 | tf_op jit(solution)/shard_map/ppermute | solution.py:50
  249.7 75.5 %collective-permute-start.21 = (bf16[1408,256]{1,0:T(8,128)(2,1)}, bf16[1408,256]{1,0:T(8,128)(2,1)S(1)}, u32[]{:S(2)}, u32[]{:S(2)}) collective-permute-start(bf16[1408,256]{1,0:T(8,128)(2,1)} %collective-permute-done.17), channel_id=1, source_target_pairs={{0,4},{4,0},{8,12},{12,8},{16,20},{20,16},{24,28},{28,24},{1,5},{5... | collective-permute-start | bytes 2162696 | tf_op jit(solution)/shard_map/ppermute | solution.py:50
  325.6 5.8 %collective-permute-start.22 = (bf16[192,2048]{1,0:T(8,128)(2,1)S(1)}, bf16[192,2048]{1,0:T(8,128)(2,1)S(1)}, u32[]{:S(2)}, u32[]{:S(2)}) collective-permute-start(bf16[192,2048]{1,0:T(8,128)(2,1)S(1)} %fusion.65), channel_id=1, source_target_pairs={{0,1},{1,0},{2,3},{3,2},{4,5},{5,4},{6,7},{7,6},{8,9},{9,8},{10,11... | collective-permute-start | bytes 2359304 | tf_op jit(solution)/shard_map/ppermute | solution.py:50
  331.6 1.2 copy-start.1
  332.8 11.7 %collective-permute-start.23 = (bf16[96,2048]{1,0:T(8,128)(2,1)S(1)}, bf16[96,2048]{1,0:T(8,128)(2,1)}, u32[]{:S(2)}, u32[]{:S(2)}) collective-permute-start(bf16[96,2048]{1,0:T(8,128)(2,1)S(1)} %slice.169), channel_id=1, source_target_pairs={{0,2},{1,3},{2,0},{3,1},{4,6},{5,7},{6,4},{7,5},{8,10},{9,11},{10,... | collective-permute-start | bytes 1179656 | tf_op jit(solution)/shard_map/ppermute | solution.py:50
  333.8 12.2 %copy-start.4 = (bf16[96,2048]{1,0:T(8,128)(2,1)S(1)}, bf16[96,2048]{1,0:T(8,128)(2,1)}, u32[]{:S(2)}) copy-start(bf16[96,2048]{1,0:T(8,128)(2,1)} %copy-done.3) | copy-start | bytes 1179652
Sparse Core Ops, SparseCore 0:
  9.5 100.6 all-gather.1
